TPU v7x, 32 devices: a whole 2x2x4 slice. The times are simulated.
32 devices in a mesh: ep: 8 (over z, x), tp: 4 (over y, core).
Axes of the slice: x: 2, y: 2, z: 4, core: 2. Of those that a mesh axis runs over, the one named last changes fastest.
Arguments:
- queries: bfloat16 [8192, 512], P('ep', 'tp'), may hold values from -6 to 6
- head_key_rows: bfloat16 [8192, 512], P('ep', 'tp'), may hold values from -6 to 6
- head_value_rows: bfloat16 [8192, 1024], P('ep', 'tp'), may hold values from -18 to 18
- log_input_gate: float32 [8192, 8], P('ep', 'tp'), may hold values from -6 to 120
- forget_logits: float32 [8192, 8], P('ep', 'tp'), may hold values from -8 to 8
- head_forget_bias: float32 [8], P('tp'), may hold values from 3 to 20
- extra_log_forget: float32 [8192, 8], P('ep', 'tp'), may hold values from -1 to 0
- output_gate_logits: bfloat16 [8192, 1024], P('ep', 'tp'), may hold values from -6 to 6
- head_norm_gain: float32 [1024], P('tp'), may hold values from 0.1 to 1.9
- mixer_output_weight: bfloat16 [1024, 2048], replicated, may hold values from -0.1875 to 0.1875
- second_batch_input: bfloat16 [6144, 2048], P(('ep', 'tp')), may hold values from -6 to 6
- expert_norm_gain: float32 [2048], replicated, may hold values from 0.1 to 1.9
- routed_expert_index: int32 [6144, 2], P(('ep', 'tp')), may hold values from 0 to 31, all different within a row; in each aligned block of 192 rows (0 to 191, 192 to 383, ...) at most 18 rows name the same one
- routed_copy_weight: float32 [6144, 2], P(('ep', 'tp')), may hold values from 0.3 to 1.5
- routed_gate_weight: bfloat16 [32, 2048, 1024], P(('ep', 'tp')), may hold values from -0.125 to 0.125
- routed_up_weight: bfloat16 [32, 2048, 1024], P(('ep', 'tp')), may hold values from -0.125 to 0.125
- routed_down_weight: bfloat16 [32, 1024, 2048], P(('ep', 'tp')), may hold values from -0.1875 to 0.1875
- shared_gate_weight: bfloat16 [2048, 384], replicated, may hold values from -0.125 to 0.125
- shared_up_weight: bfloat16 [2048, 384], replicated, may hold values from -0.125 to 0.125
- shared_down_weight: bfloat16 [384, 2048], replicated, may hold values from -0.3125 to 0.3125
Outputs:
- mixer_first_output: bfloat16 [8192, 2048], P(('ep', 'tp'))
- moe_out: bfloat16 [6144, 2048], P(('ep', 'tp'))
Inputs may be any that keep to these rules, and one draw needn't show every extreme that they name: `routed_expert_index`: in each aligned block of 192 rows (the rows of one device) no expert is named by more than 18 rows, and in some blocks one expert is named by exactly 18; every expert is named somewhere.
All inputs are finite; a program needn't handle non-finite values.
Results may differ from a plain program's by a relative error of at most 0.0068.
Values may be sent and summed in bfloat16 or wider, within the bound.
A program may use at most 128 MiB of HBM per device.

v0:
```python
import jax
import jax.numpy as jnp
from jax import lax
from jax.experimental import pallas as pl
from jax.experimental.pallas import tpu as pltpu
from jax.sharding import PartitionSpec as P

BLK = 128


F32 = jnp.float32
BF16 = jnp.bfloat16
LANE_ROWS = 16
CHUNKS = 2


def mm(left, right):
    return jnp.dot(left, right, preferred_element_type=F32)


def iota(shape, axis):
    return lax.broadcasted_iota(jnp.int32, shape, axis)


def moe_body(ep_count, tp_count, capacity, refs, mixer):
    (x_ref, gain_ref, idx_ref, idx_t_ref, weight_ref, wg_hbm, wu_hbm, wd_hbm, sg_hbm, su_hbm,
     sd_hbm, out_ref, normed, send, recv, ysend, ret, wg, wu, wd, sg, su, sd, xc, hc, yc, shared,
     load_sem, go_send, go_recv, back_send, back_recv) = refs
    count = ep_count * tp_count
    tokens, width = x_ref.shape
    hidden_width = wg.shape[1]
    shared_width = sg.shape[1]
    groups = capacity // LANE_ROWS
    tail = capacity - groups * LANE_ROWS
    parts = LANE_ROWS // tail
    piece = width // parts
    base = groups * width
    chunks = CHUNKS
    sources = count // chunks
    main_rows = sources * LANE_ROWS
    tail_rows = sources * tail
    me = lax.axis_index("ep") * tp_count + lax.axis_index("tp")

    def device(index):
        return (index // tp_count, lax.rem(index, tp_count))

    def rows_of(index):
        return pl.ds(pl.multiple_of(index * LANE_ROWS, LANE_ROWS), LANE_ROWS)

    loads = [
        pltpu.make_async_copy(source, target, load_sem.at[number])
        for number, (source, target) in enumerate(
            [(sg_hbm, sg), (su_hbm, su), (sd_hbm, sd),
             (wg_hbm.at[0], wg), (wu_hbm.at[0], wu), (wd_hbm.at[0], wd)]
        )
    ]
    for load in loads:
        load.start()

    barrier = pltpu.get_barrier_semaphore()

    def greet(step, carry):
        pl.semaphore_signal(
            barrier, inc=1, device_id=device(lax.rem(me + step, count)),
            device_id_type=pl.DeviceIdType.MESH,
        )
        return carry

    lax.fori_loop(1, count, greet, 0)

    floats = x_ref[...].astype(F32)
    inverse = lax.rsqrt(jnp.mean(floats * floats, axis=1, keepdims=True) + 1e-6)
    normed[...] = (floats * inverse * gain_ref[...]).astype(BF16)

    expert_rows = iota((count, tokens), 0)
    first_t = idx_t_ref[0:1, :]
    second_t = idx_t_ref[1:2, :]
    hit_first = expert_rows == first_t
    hit_second = expert_rows == second_t
    named = (hit_first | hit_second).astype(F32).astype(BF16)
    before = (iota((tokens, tokens), 0) < iota((tokens, tokens), 1)).astype(F32).astype(BF16)
    earlier = mm(named, before)
    place_first = jnp.sum(jnp.where(hit_first, earlier, 0.0), axis=0, keepdims=True)
    place_second = jnp.sum(jnp.where(hit_second, earlier, 0.0), axis=0, keepdims=True)
    place_first = place_first.astype(jnp.int32)
    place_second = place_second.astype(jnp.int32)

    def keys_main(expert, place, group):
        local = place - group * LANE_ROWS
        return jnp.where((local >= 0) & (local < LANE_ROWS), expert * LANE_ROWS + local, -1)

    def keys_tail(expert, place):
        local = place - groups * LANE_ROWS
        return jnp.where(local >= 0, expert * LANE_ROWS + local * parts, -LANE_ROWS)

    slot_rows = iota((count * LANE_ROWS, tokens), 0)
    for group in range(groups):
        pick = (slot_rows == keys_main(first_t, place_first, group)) | (
            slot_rows == keys_main(second_t, place_second, group)
        )
        pick = pick.astype(F32).astype(BF16)
        step = width // 4
        for at in range(0, width, step):
            send[:, group * width + at:group * width + at + step] = mm(
                pick, normed[:, at:at + step]
            ).astype(BF16)
    tail_first = keys_tail(first_t, place_first)
    tail_second = keys_tail(second_t, place_second)
    total = jnp.zeros((count * LANE_ROWS, piece), F32)
    for part in range(parts):
        pick = (slot_rows == tail_first + part) | (slot_rows == tail_second + part)
        total = total + mm(
            pick.astype(F32).astype(BF16), normed[:, part * piece:(part + 1) * piece]
        )
    send[:, base:base + piece] = total.astype(BF16)

    early, middle, late = mixer
    early()
    pl.semaphore_wait(barrier, count - 1)
    middle(0)

    def slot_of(distance):
        return lax.rem(distance, chunks) * sources + distance // chunks

    def go(distance):
        target = lax.rem(me + distance, count)
        return pltpu.make_async_remote_copy(
            src_ref=send.at[rows_of(target), :],
            dst_ref=recv.at[rows_of(slot_of(distance)), :],
            send_sem=go_send.at[distance],
            recv_sem=go_recv.at[distance],
            device_id=device(target),
            device_id_type=pl.DeviceIdType.MESH,
        )

    def back(distance):
        target = lax.rem(me - distance + count, count)
        return pltpu.make_async_remote_copy(
            src_ref=ysend.at[rows_of(slot_of(distance)), :],
            dst_ref=ret.at[rows_of(me), :],
            send_sem=back_send.at[distance],
            recv_sem=back_recv.at[distance],
            device_id=device(target),
            device_id_type=pl.DeviceIdType.MESH,
        )

    def each(low, high, stride, work):
        def turn(step, carry):
            work(low + step * stride)
            return carry

        lax.fori_loop(0, -(-(high - low) // stride), turn, 0)

    each(1, count, 1, lambda distance: go(distance).start())
    recv[0:LANE_ROWS, :] = send[rows_of(me), :]

    middle(1)

    for load in loads[:3]:
        load.wait()
    gate = mm(normed[...], sg[...])
    hidden = (gate * jax.nn.sigmoid(gate) * mm(normed[...], su[...])).astype(BF16)
    for at in range(0, width, width // 4):
        shared[:, at:at + width // 4] = mm(hidden, sd[:, at:at + width // 4])
    for load in loads[3:]:
        load.wait()

    def select(part, transposed):
        shape = (main_rows, tail_rows) if transposed else (tail_rows, main_rows)
        axis = 1 if transposed else 0
        chosen = iota(shape, 1 - axis) == iota(shape, axis) * parts + part
        return chosen.astype(F32).astype(BF16)

    for chunk in range(chunks):
        each(chunk if chunk else chunks, count, chunks, lambda distance: go(distance).wait_recv())
        low = chunk * main_rows
        for group in range(groups):
            xc[group * main_rows:(group + 1) * main_rows, :] = recv[
                low:low + main_rows, group * width:(group + 1) * width
            ]
        start = groups * main_rows
        for part in range(parts):
            xc[start:start + tail_rows, part * piece:(part + 1) * piece] = mm(
                select(part, False), recv[low:low + main_rows, base:base + piece]
            ).astype(BF16)

        @pl.loop(0, hidden_width // 256)
        def _(turn):
            columns = pl.ds(pl.multiple_of(turn * 256, 256), 256)
            gate = mm(xc[...], wg[:, columns])
            up = mm(xc[...], wu[:, columns])
            hc[:, columns] = (gate * jax.nn.sigmoid(gate) * up).astype(BF16)

        @pl.loop(0, width // 256)
        def _(turn):
            columns = pl.ds(pl.multiple_of(turn * 256, 256), 256)
            yc[:, columns] = mm(hc[...], wd[:, columns]).astype(BF16)

        for group in range(groups):
            ysend[low:low + main_rows, group * width:(group + 1) * width] = yc[
                group * main_rows:(group + 1) * main_rows, :
            ]
        total = jnp.zeros((main_rows, piece), F32)
        for part in range(parts):
            total = total + mm(
                select(part, True),
                yc[start:start + tail_rows, part * piece:(part + 1) * piece],
            )
        ysend[low:low + main_rows, base:base + piece] = total.astype(BF16)
        each(chunk if chunk else chunks, count, chunks, lambda distance: back(distance).start())
    ret[rows_of(me), :] = ysend[0:LANE_ROWS, :]
    late()

    first = idx_ref[:, 0:1]
    second = idx_ref[:, 1:2]
    expert_lanes = iota((tokens, count), 1)
    hit_first = expert_lanes == first
    hit_second = expert_lanes == second
    named = (hit_first | hit_second).astype(F32).astype(BF16)
    after = (iota((tokens, tokens), 1) < iota((tokens, tokens), 0)).astype(F32).astype(BF16)
    earlier = mm(after, named)
    place_first = jnp.sum(jnp.where(hit_first, earlier, 0.0), axis=1, keepdims=True)
    place_second = jnp.sum(jnp.where(hit_second, earlier, 0.0), axis=1, keepdims=True)
    place_first = place_first.astype(jnp.int32)
    place_second = place_second.astype(jnp.int32)
    slot_lanes = iota((tokens, count * LANE_ROWS), 1)

    def mixing(first_key, second_key):
        values = jnp.where(slot_lanes == first_key, weight_ref[:, 0:1], 0.0) + jnp.where(
            slot_lanes == second_key, weight_ref[:, 1:2], 0.0
        )
        high = values.astype(BF16)
        return high, (values - high.astype(F32)).astype(BF16)

    main_mix = [
        mixing(keys_main(first, place_first, group), keys_main(second, place_second, group))
        for group in range(groups)
    ]
    each(1, count, 1, lambda distance: back(distance).wait_recv())
    tail_first = keys_tail(first, place_first)
    tail_second = keys_tail(second, place_second)
    for part in range(parts):
        columns = slice(part * piece, (part + 1) * piece)
        total = shared[:, columns]
        for group in range(groups):
            values = ret[:, group * width + part * piece:group * width + (part + 1) * piece]
            high, low = main_mix[group]
            total = total + (mm(high, values) + mm(low, values))
        values = ret[:, base:base + piece]
        high, low = mixing(tail_first + part, tail_second + part)
        total = total + (mm(high, values) + mm(low, values))
        out_ref[:, columns] = total.astype(BF16)
    each(1, count, 1, lambda distance: go(distance).wait_send())
    each(1, count, 1, lambda distance: back(distance).wait_send())


STATE_ROWS = 8


def nt(left, right, precision=None):
    return lax.dot_general(
        left, right, (((1,), (1,)), ((), ())), precision=precision, preferred_element_type=F32
    )


def halves(value):
    high = value.astype(BF16)
    return high, (value - high.astype(F32)).astype(BF16)


def log_one_plus(small):
    series = small * (1.0 - small * (0.5 - small * (1.0 / 3.0 - small * 0.25)))
    return jnp.where(small < 0.01, series, jnp.log(1.0 + small))


def mixer_parts(ep_count, tp_count, refs):
    (q_ref, k_ref, v_ref, in_ref, forget_ref, bias_ref, extra_ref, gate_ref, gain_ref, wo_hbm,
     out_ref, wo, locals_ref, state_send, state_recv, incoming, incoming_max, u_ref, squares_ref,
     u_recv, squares_recv, wo_sem, st_send, st_recv, us_send, us_recv, sq_send, sq_recv) = refs
    exact = lax.Precision.HIGHEST
    heads, length = in_ref.shape
    blocks = length // BLK
    key_dim = q_ref.shape[1] // heads
    value_dim = v_ref.shape[1] // heads
    own_width = heads * value_dim
    scale = key_dim ** (-0.5)
    message = key_dim + STATE_ROWS
    share = length // tp_count
    share_blocks = share // BLK
    ep_at = lax.axis_index("ep")
    tp_at = lax.axis_index("tp")
    load = pltpu.make_async_copy(wo_hbm, wo, wo_sem)

    def block_rows(ref, transform=lambda value, head: value):
        whole = ref[...]
        return jnp.concatenate(
            [
                transform(whole[head:head + 1, at * BLK:(at + 1) * BLK], head)
                for head in range(heads)
                for at in range(blocks)
            ],
            axis=0,
        )

    def key_block(head, at):
        return k_ref[at * BLK:(at + 1) * BLK, head * key_dim:(head + 1) * key_dim]

    def wide_values(head, at):
        values = v_ref[at * BLK:(at + 1) * BLK, head * value_dim:(head + 1) * value_dim]
        return jnp.concatenate([values, jnp.ones((BLK, value_dim), BF16)], axis=1)

    found = {}

    def grow(state, number):
        memory, top = state
        total = found["total"][number:number + 1, :]
        block_top = found["block_top"][number:number + 1, :]
        new_top = jnp.maximum(top + total, block_top)
        memory = jnp.exp(top + total - new_top) * memory + jnp.exp(
            block_top - new_top
        ) * locals_ref[number]
        return memory, new_top

    def diagonal():
        shape = (key_dim, value_dim)
        return iota(shape, 0) == iota(shape, 1)

    def early():
        load.start()
        logits = block_rows(forget_ref, lambda value, head: value + bias_ref[head:head + 1, :])
        kept = jnp.minimum(logits, 0.0) - log_one_plus(jnp.exp(-jnp.abs(logits)))
        kept = kept + block_rows(extra_ref)
        gates = block_rows(in_ref)
        upper = (iota((BLK, BLK), 0) <= iota((BLK, BLK), 1)).astype(F32)
        cumulative = jnp.dot(kept, upper, precision=exact, preferred_element_type=F32)
        total = cumulative[:, BLK - 1:BLK]
        gap = total - cumulative + gates
        block_top = jnp.max(gap, axis=1, keepdims=True)
        weight = jnp.exp(gap - block_top)
        found["total"], found["block_top"] = total, block_top
        found["cumulative"], found["shift"] = cumulative, gates - cumulative
        eye = (iota((key_dim, key_dim), 0) == iota((key_dim, key_dim), 1)).astype(F32).astype(BF16)
        for head in range(heads):
            state = (
                jnp.zeros((key_dim, 2 * value_dim), F32), jnp.full((1, 1), -1e30, F32)
            )
            decay = jnp.zeros((1, 1), F32)
            for at in range(blocks):
                number = head * blocks + at
                turned = nt(eye, key_block(head, at)) * weight[number:number + 1, :]
                high, low = halves(turned)
                values = wide_values(head, at)
                locals_ref[number] = mm(high, values) + mm(low, values)
                state = grow(state, number)
                decay = decay + total[number:number + 1, :]
            memory, top = state
            low_row = head * message
            state_send[low_row:low_row + key_dim, :] = memory[:, :value_dim]
            norm = jnp.sum(
                jnp.where(diagonal(), memory[:, value_dim:], 0.0), axis=0, keepdims=True
            )
            row = iota((STATE_ROWS, value_dim), 0)
            state_send[low_row + key_dim:low_row + message, :] = jnp.where(
                row == 0, norm, jnp.where(row == 1, top, decay)
            )

    def state_copy(distance):
        return pltpu.make_async_remote_copy(
            src_ref=state_send,
            dst_ref=state_recv.at[distance],
            send_sem=st_send.at[distance],
            recv_sem=st_recv.at[distance],
            device_id=(ep_at + distance, tp_at),
            device_id_type=pl.DeviceIdType.MESH,
        )

    def u_copies(distance):
        target = lax.rem(tp_at + distance, tp_count)
        place = pl.ds(pl.multiple_of(tp_at * own_width, own_width), own_width)
        return [
            pltpu.make_async_remote_copy(
                src_ref=u_ref.at[pl.ds(pl.multiple_of(target * share, share), share), :],
                dst_ref=u_recv.at[:, place],
                send_sem=us_send.at[distance],
                recv_sem=us_recv.at[distance],
                device_id=(ep_at, target),
                device_id_type=pl.DeviceIdType.MESH,
            ),
            pltpu.make_async_remote_copy(
                src_ref=squares_ref.at[target],
                dst_ref=squares_recv.at[distance],
                send_sem=sq_send.at[distance],
                recv_sem=sq_recv.at[distance],
                device_id=(ep_at, target),
                device_id_type=pl.DeviceIdType.MESH,
            ),
        ]

    def later_exists(distance):
        return ep_at + distance < ep_count

    def middle(stage):
        if stage == 0:
            for distance in range(1, ep_count):
                @pl.when(later_exists(distance))
                def _():
                    state_copy(distance).start()
            return
        incoming[...] = jnp.zeros_like(incoming)
        incoming_max[...] = jnp.full_like(incoming_max, -1e30)
        for distance in range(ep_count - 1, 0, -1):
            @pl.when(ep_at >= distance)
            def _():
                state_copy(distance).wait_recv()
                for head in range(heads):
                    low_row = head * message
                    memory = state_recv[distance, low_row:low_row + key_dim, :]
                    extra = state_recv[distance, low_row + key_dim:low_row + message, :]
                    norm = jnp.sum(
                        jnp.where(diagonal(), extra[0:1, :], 0.0), axis=1, keepdims=True
                    )
                    top, decay = extra[1:2, :], extra[2:3, :]
                    old_top = incoming_max[head, 0:1, :]
                    new_top = jnp.maximum(old_top + decay, top)
                    left = jnp.exp(old_top + decay - new_top)
                    right = jnp.exp(top - new_top)
                    incoming[head, :, :value_dim] = (
                        left * incoming[head, :, :value_dim] + right * memory
                    )
                    incoming[head, :, value_dim:] = (
                        left * incoming[head, :, value_dim:] + right * norm
                    )
                    incoming_max[head] = jnp.broadcast_to(new_top, incoming_max.shape[1:])
        lower = iota((BLK, BLK), 0) >= iota((BLK, BLK), 1)
        states = [(incoming[head], incoming_max[head, 0:1, 0:1]) for head in range(heads)]
        columns = jnp.transpose(found["cumulative"])
        ones = jnp.ones((STATE_ROWS, value_dim), F32)
        for at in range(blocks):
            squares = jnp.zeros((STATE_ROWS, BLK), F32)
            for head in range(heads):
                number = head * blocks + at
                memory, top = states[head]
                query = q_ref[at * BLK:(at + 1) * BLK, head * key_dim:(head + 1) * key_dim]
                column = columns[:, number:number + 1]
                gap = jnp.where(
                    lower, column + found["shift"][number:number + 1, :], -jnp.inf
                )
                carried = column + top
                stabilizer = jnp.maximum(carried, jnp.max(gap, axis=1, keepdims=True))
                scores = nt(query, key_block(head, at)) * scale * jnp.exp(gap - stabilizer)
                high, low = halves(scores)
                values = wide_values(head, at)
                sums = mm(high, values) + mm(low, values)
                high, low = halves(memory)
                sums = sums + (jnp.exp(carried - stabilizer) * scale) * (
                    mm(query, high) + mm(query, low)
                )
                hidden = sums[:, :value_dim] / jnp.maximum(
                    jnp.abs(sums[:, value_dim:]), jnp.exp(-stabilizer)
                )
                squares = squares + nt(ones, hidden * hidden, exact)
                place = slice(head * value_dim, (head + 1) * value_dim)
                gate = gate_ref[at * BLK:(at + 1) * BLK, place].astype(F32)
                u_ref[at * BLK:(at + 1) * BLK, place] = (
                    hidden * gain_ref[:, place] * jax.nn.sigmoid(gate)
                ).astype(BF16)
                states[head] = grow(states[head], number)
            squares_ref[at // share_blocks, at % share_blocks] = squares
        for distance in range(1, tp_count):
            for copy in u_copies(distance):
                copy.start()
        place = pl.ds(pl.multiple_of(tp_at * own_width, own_width), own_width)
        u_recv[:, place] = u_ref[pl.ds(pl.multiple_of(tp_at * share, share), share), :]
        squares_recv[0] = squares_ref[tp_at]

    def late():
        for distance in range(1, tp_count):
            for copy in u_copies(distance):
                copy.wait_recv()
        squares = squares_recv[0]
        for distance in range(1, tp_count):
            squares = squares + squares_recv[distance]
        inverse_row = lax.rsqrt(squares / (heads * tp_count * value_dim) + 1e-6)
        eye = (iota((BLK, BLK), 0) == iota((BLK, BLK), 1)).astype(F32)
        load.wait()
        width = wo.shape[1]
        for at in range(share_blocks):
            inverse = nt(eye, inverse_row[at], exact)[:, 0:1]

            @pl.loop(0, width // 512)
            def _(turn):
                place = pl.ds(pl.multiple_of(turn * 512, 512), 512)
                product = mm(u_recv[at * BLK:(at + 1) * BLK, :], wo[:, place])
                out_ref[at * BLK:(at + 1) * BLK, place] = (product * inverse).astype(BF16)

        for distance in range(1, ep_count):
            @pl.when(later_exists(distance))
            def _():
                state_copy(distance).wait_send()
        for distance in range(1, tp_count):
            for copy in u_copies(distance):
                copy.wait_send()

    return early, middle, late


def on_device(
    queries,
    head_key_rows,
    head_value_rows,
    log_input_gate,
    forget_logits,
    head_forget_bias,
    extra_log_forget,
    output_gate_logits,
    head_norm_gain,
    mixer_output_weight,
    second_batch_input,
    expert_norm_gain,
    routed_expert_index,
    routed_copy_weight,
    routed_gate_weight,
    routed_up_weight,
    routed_down_weight,
    shared_gate_weight,
    shared_up_weight,
    shared_down_weight,
):
    tokens, width = second_batch_input.shape
    ep_count = lax.axis_size("ep")
    tp_count = lax.axis_size("tp")
    count = ep_count * tp_count
    top_count = routed_expert_index.shape[1]
    capacity = max(2, 3 * tokens * top_count // (2 * count))
    wire = capacity * width // LANE_ROWS
    rows = count // CHUNKS * capacity
    hidden_width = routed_gate_weight.shape[2]
    length = queries.shape[0]
    heads = head_forget_bias.shape[0]
    key_dim = queries.shape[1] // heads
    value_dim = head_value_rows.shape[1] // heads
    blocks = length // BLK
    share = length // tp_count
    dma = pltpu.SemaphoreType.DMA
    vmem = pl.BlockSpec(memory_space=pltpu.VMEM)
    hbm = pl.BlockSpec(memory_space=pl.ANY)

    moe_scratch = (
        [pltpu.VMEM((tokens, width), BF16)]
        + [pltpu.VMEM((count * LANE_ROWS, wire), BF16)] * 4
        + [
            pltpu.VMEM(array.shape[-2:], BF16)
            for array in (
                routed_gate_weight, routed_up_weight, routed_down_weight,
                shared_gate_weight, shared_up_weight, shared_down_weight,
            )
        ]
        + [
            pltpu.VMEM((rows, width), BF16),
            pltpu.VMEM((rows, hidden_width), BF16),
            pltpu.VMEM((rows, width), BF16),
            pltpu.VMEM((tokens, width), F32),
            dma((6,)), dma((count,)), dma((count,)), dma((count,)), dma((count,)),
        ]
    )
    message = heads * (key_dim + STATE_ROWS)
    mixer_scratch = [
        pltpu.VMEM(mixer_output_weight.shape, BF16),
        pltpu.VMEM((heads * blocks, key_dim, 2 * value_dim), F32),
        pltpu.VMEM((message, value_dim), F32),
        pltpu.VMEM((ep_count, message, value_dim), F32),
        pltpu.VMEM((heads, key_dim, 2 * value_dim), F32),
        pltpu.VMEM((heads, STATE_ROWS, value_dim), F32),
        pltpu.VMEM((length, heads * value_dim), BF16),
        pltpu.VMEM((tp_count, share // BLK, STATE_ROWS, BLK), F32),
        pltpu.VMEM((share, tp_count * heads * value_dim), BF16),
        pltpu.VMEM((tp_count, share // BLK, STATE_ROWS, BLK), F32),
        dma, dma((ep_count,)), dma((ep_count,)),
        dma((tp_count,)), dma((tp_count,)), dma((tp_count,)), dma((tp_count,)),
    ]

    def kernel(*refs):
        mixer_in, moe_in = refs[:10], refs[10:21]
        mixer_out, moe_out = refs[21], refs[22]
        scratch = refs[23:]
        cut = len(moe_scratch)
        mixer = mixer_parts(ep_count, tp_count, (*mixer_in, mixer_out, *scratch[cut:]))
        moe_body(ep_count, tp_count, capacity, (*moe_in, moe_out, *scratch[:cut]), mixer)

    return pl.pallas_call(
        kernel,
        out_shape=(
            jax.ShapeDtypeStruct((share, width), BF16),
            jax.ShapeDtypeStruct((tokens, width), BF16),
        ),
        in_specs=[vmem] * 9 + [hbm] + [vmem] * 5 + [hbm] * 6,
        out_specs=(vmem, vmem),
        scratch_shapes=moe_scratch + mixer_scratch,
        compiler_params=pltpu.CompilerParams(
            collective_id=0, has_side_effects=True, vmem_limit_bytes=62 * 1024 * 1024
        ),
        name="both",
    )(
        queries, head_key_rows, head_value_rows, log_input_gate.T, forget_logits.T,
        head_forget_bias[:, None], extra_log_forget.T, output_gate_logits,
        head_norm_gain[None, :], mixer_output_weight,
        second_batch_input, expert_norm_gain[None, :], routed_expert_index,
        routed_expert_index.T, routed_copy_weight, routed_gate_weight, routed_up_weight,
        routed_down_weight, shared_gate_weight, shared_up_weight, shared_down_weight,
    )


def solution(mesh):
    in_specs = (
        P("ep", "tp"),
        P("ep", "tp"),
        P("ep", "tp"),
        P("ep", "tp"),
        P("ep", "tp"),
        P("tp"),
        P("ep", "tp"),
        P("ep", "tp"),
        P("tp"),
        P(),
        P(("ep", "tp"), None),
        P(),
        P(("ep", "tp"), None),
        P(("ep", "tp"), None),
        P(("ep", "tp"), None, None),
        P(("ep", "tp"), None, None),
        P(("ep", "tp"), None, None),
        P(),
        P(),
        P(),
    )
    out_specs = (P(("ep", "tp"), None), P(("ep", "tp"), None))
    return jax.shard_map(
        on_device, mesh=mesh, in_specs=in_specs, out_specs=out_specs, check_vma=False
    )
```

profile of v0, /device:TPU:0, one launch (start us, length us, event | category | flops | bytes accessed | tf_op | source)
XLA Modules:
  0.0 167.9 jit_solution(515552314508276072)
XLA Ops:
  0.6 1.3 copy.22.refs_5_
  2.0 1.4 copy.24.refs_14_
  3.4 1.4 copy.23.refs_12_
  4.8 158.7 %both.1 = (bf16[256,2048]{1,0:T(8,128)(2,1)}, bf16[192,2048]{1,0:T(8,128)(2,1)}) custom-call(bf16[1024,128]{1,0:T(8,128)(2,1)} %refs_0_.1, bf16[1024,128]{1,0:T(8,128)(2,1)} %refs_1_.1, bf16[1024,256]{1,0:T(8,128)(2,1)} %refs_2_.1, f32[2,1024]{1,0:T(2,128)} %bitcast.7, f32[2,1024]{1,0:T(2,128)} %bitcast.8, f32[2,1]{1,0:T(2,128)} %copy.22.refs_5_, ...), custom_call_target="tpu_custom_call" | custom-call | tf_op jit(solution)/shard_map/both/pallas_call | solution.py:590
  163.5 2.3 %copy.27 = bf16[256,2048]{1,0:T(8,128)(2,1)} copy(bf16[256,2048]{1,0:T(8,128)(2,1)} %get-tuple-element.4) | data formatting | bytes 2097152
  165.9 2.1 %copy.28 = bf16[192,2048]{1,0:T(8,128)(2,1)} copy(bf16[192,2048]{1,0:T(8,128)(2,1)} %get-tuple-element.5) | data formatting | bytes 1572864
where the time goes:
time: 168 us
  Pallas kernels  159 us (95%)
  local copies, waits for them, and re-layouts  8.6 us (5%)
    pallas_call x1, Pallas kernels, on_device(): pl.pallas_call(kernel, out_shape=(jax.ShapeDtypeStruct((share, width), BF...  159 us
    unnamed x4, local copies, waits for them, and re-layouts  7.28 us

commit v1 on v0

v1 whole, which is shorter than its diff:
```python
import jax
import jax.numpy as jnp
from jax import lax
from jax.experimental import pallas as pl
from jax.experimental.pallas import tpu as pltpu
from jax.sharding import PartitionSpec as P

BLK = 128


F32 = jnp.float32
BF16 = jnp.bfloat16
LANE_ROWS = 16
CORES = 2
PIECES = 2


def mm(left, right):
    return jnp.dot(left, right, preferred_element_type=F32)


def iota(shape, axis):
    return lax.broadcasted_iota(jnp.int32, shape, axis)


class Place:
    def __init__(self, ep_count, tp_count):
        self.side = max(1, tp_count // CORES)
        self.tp_count = tp_count
        self.planes = ep_count // self.side
        self.depth = self.planes // 2
        self.cell = self.side * tp_count
        self.near = self.depth * self.cell
        self.ep_at = lax.axis_index("ep")
        self.tp_at = lax.axis_index("tp")
        plane = self.ep_at // self.side
        self.row = lax.rem(self.ep_at, self.side)
        self.half = plane // self.depth
        self.level = plane - self.half * self.depth
        self.stage = self.half * self.level + (1 - self.half) * (self.depth - 1 - self.level)
        self.spot = self.level * self.cell + self.row * tp_count + self.tp_at
        self.partner = ((self.planes - 1 - plane) * self.side + self.row, self.tp_at)

    def at(self, level, row, tp):
        device = ((self.half * self.depth + level) * self.side + row, tp)
        return device, level * self.cell + row * self.tp_count + tp

    def across(self, step, sign):
        row_step, tp_step = step // self.tp_count, lax.rem(step, self.tp_count)
        row = lax.rem(self.row + sign * row_step + self.side, self.side)
        tp = lax.rem(self.tp_at + sign * tp_step + self.tp_count, self.tp_count)
        return row, tp

    def away(self, distance, sign):
        level_step = distance // self.cell
        level = lax.rem(self.level + sign * level_step + self.depth, self.depth)
        return self.at(level, *self.across(lax.rem(distance, self.cell), sign))

    def level_of(self, stage):
        return self.half * stage + (1 - self.half) * (self.depth - 1 - stage)


def each(low, high, work):
    def turn(step, carry):
        work(step)
        return carry

    lax.fori_loop(low, high, turn, 0)


def rows_of(index):
    return pl.ds(pl.multiple_of(index * LANE_ROWS, LANE_ROWS), LANE_ROWS)


def remote(source, target, send_sem, recv_sem, device):
    return pltpu.make_async_remote_copy(
        src_ref=source, dst_ref=target, send_sem=send_sem, recv_sem=recv_sem,
        device_id=device, device_id_type=pl.DeviceIdType.MESH,
    )


def as_weight(mask):
    return mask.astype(F32).astype(BF16)


class Experts:
    def __init__(self, place, capacity, refs):
        (self.x_ref, self.gain_ref, self.idx_ref, self.weight_ref, wg_hbm, wu_hbm, wd_hbm, sg_hbm,
         su_hbm, sd_hbm, self.out_ref, self.normed, self.meta, self.far_block, self.far_meta,
         self.send_own, self.send_far, self.recv, self.ysend, self.ret_own, self.ret_far,
         self.far_out, self.far_in, self.wg, self.wu, self.wd, self.sg, self.su, self.sd, self.xc,
         self.hc, self.yc, self.total, load_sem, self.go_send, self.go_recv, self.back_send,
         self.back_recv, self.over_send, self.over_recv) = refs
        self.place = place
        self.tokens, self.width = self.x_ref.shape
        self.groups = capacity // LANE_ROWS
        self.tail = capacity - self.groups * LANE_ROWS
        self.parts = LANE_ROWS // self.tail
        self.piece = self.width // self.parts
        self.base = self.groups * self.width
        self.loads = [
            pltpu.make_async_copy(source, target, load_sem.at[number])
            for number, (source, target) in enumerate(
                [(sg_hbm, self.sg), (su_hbm, self.su), (sd_hbm, self.sd),
                 (wg_hbm.at[0], self.wg), (wu_hbm.at[0], self.wu), (wd_hbm.at[0], self.wd)]
            )
        ]

    def open(self):
        place, tokens = self.place, self.tokens
        for load in self.loads:
            load.start()
        barrier = pltpu.get_barrier_semaphore()

        def greet(device):
            pl.semaphore_signal(
                barrier, inc=1, device_id=device, device_id_type=pl.DeviceIdType.MESH
            )

        each(1, place.near, lambda distance: greet(place.away(distance, 1)[0]))
        greet(place.partner)

        floats = self.x_ref[...].astype(F32)
        inverse = lax.rsqrt(jnp.mean(floats * floats, axis=1, keepdims=True) + 1e-6)
        self.normed[...] = (floats * inverse * self.gain_ref[...]).astype(BF16)

        expert_rows = iota((2 * place.near, tokens), 0)
        first, second = self.idx_ref[0:1, :], self.idx_ref[1:2, :]
        hit_first = expert_rows == first
        hit_second = expert_rows == second
        named = as_weight(hit_first | hit_second)
        before = as_weight(iota((tokens, tokens), 0) < iota((tokens, tokens), 1))
        earlier = mm(named, before)
        self.meta[...] = jnp.zeros_like(self.meta)
        self.meta[0:1, :tokens] = first.astype(F32)
        self.meta[1:2, :tokens] = second.astype(F32)
        self.meta[2:3, :tokens] = jnp.sum(jnp.where(hit_first, earlier, 0.0), axis=0, keepdims=True)
        self.meta[3:4, :tokens] = jnp.sum(
            jnp.where(hit_second, earlier, 0.0), axis=0, keepdims=True
        )
        self.meta[4:6, :tokens] = self.weight_ref[...]
        self.slots(self.normed, self.meta, self.send_own)
        pl.semaphore_wait(barrier, place.near)

    def keys(self, first, second, place_first, place_second):
        near, low = self.place.near, self.place.half * self.place.near

        def main(expert, place, group):
            local, near_expert = place - group * LANE_ROWS, expert - low
            inside = (near_expert >= 0) & (near_expert < near)
            inside = inside & (local >= 0) & (local < LANE_ROWS)
            return jnp.where(inside, near_expert * LANE_ROWS + local, -LANE_ROWS)

        def tail(expert, place):
            local, near_expert = place - self.groups * LANE_ROWS, expert - low
            inside = (near_expert >= 0) & (near_expert < near) & (local >= 0)
            return jnp.where(inside, near_expert * LANE_ROWS + local * self.parts, -LANE_ROWS)

        mains = [
            (main(first, place_first, group), main(second, place_second, group))
            for group in range(self.groups)
        ]
        return mains, (tail(first, place_first), tail(second, place_second))

    def slots(self, block, meta, send):
        whole = meta[:, :self.tokens].astype(jnp.int32)
        mains, tails = self.keys(*[whole[row:row + 1, :] for row in range(4)])
        slot_rows = iota((self.place.near * LANE_ROWS, self.tokens), 0)
        step = self.width // 4
        for group, (first, second) in enumerate(mains):
            pick = as_weight((slot_rows == first) | (slot_rows == second))
            for at in range(0, self.width, step):
                send[:, group * self.width + at:group * self.width + at + step] = mm(
                    pick, block[:, at:at + step]
                ).astype(BF16)
        total = jnp.zeros((self.place.near * LANE_ROWS, self.piece), F32)
        for part in range(self.parts):
            pick = as_weight((slot_rows == tails[0] + part) | (slot_rows == tails[1] + part))
            total = total + mm(pick, block[:, part * self.piece:(part + 1) * self.piece])
        send[:, self.base:self.base + self.piece] = total.astype(BF16)

    def over(self, source, target, first):
        step = self.width // PIECES
        return [
            remote(
                source.at[:, number * step:(number + 1) * step],
                target.at[:, number * step:(number + 1) * step],
                self.over_send.at[first + number], self.over_recv.at[first + number],
                self.place.partner,
            )
            for number in range(PIECES)
        ]

    def block_copies(self):
        return [
            remote(
                self.meta, self.far_meta, self.over_send.at[2 * PIECES],
                self.over_recv.at[2 * PIECES], self.place.partner,
            )
        ] + self.over(self.normed, self.far_block, 0)

    def back_copies(self):
        return self.over(self.far_out, self.far_in, PIECES)

    def go_own(self, distance):
        device, spot = self.place.away(distance, 1)
        return remote(
            self.send_own.at[rows_of(spot), :], self.recv.at[rows_of(distance), :],
            self.go_send.at[distance], self.go_recv.at[distance], device,
        )

    def back_own(self, distance):
        device, _ = self.place.away(distance, -1)
        return remote(
            self.ysend.at[rows_of(distance), :], self.ret_own.at[rows_of(self.place.spot), :],
            self.back_send.at[distance], self.back_recv.at[distance], device,
        )

    def go_far(self, turn):
        place = self.place
        level, step = turn // place.cell, lax.rem(turn, place.cell)
        device, spot = place.at(level, *place.across(step, 1))
        slot = place.near + place.stage * place.cell + step
        return remote(
            self.send_far.at[rows_of(spot), :], self.recv.at[rows_of(slot), :],
            self.go_send.at[place.near + turn], self.go_recv.at[slot], device,
        )

    def got_far(self, stage, step):
        slot = self.place.near + stage * self.place.cell + step
        return remote(
            self.send_far.at[rows_of(0), :], self.recv.at[rows_of(slot), :],
            self.go_send.at[slot], self.go_recv.at[slot], self.place.partner,
        )

    def back_far(self, stage, step):
        place = self.place
        device, _ = place.at(place.level_of(stage), *place.across(step, -1))
        slot = place.near + stage * place.cell + step
        return remote(
            self.ysend.at[rows_of(slot), :], self.ret_far.at[rows_of(place.spot), :],
            self.back_send.at[slot],
            self.back_recv.at[place.near + place.level * place.cell + step], device,
        )

    def returned_far(self, turn):
        place = self.place
        level, step = turn // place.cell, lax.rem(turn, place.cell)
        _, spot = place.at(level, *place.across(step, 1))
        return remote(
            self.ysend.at[rows_of(0), :], self.ret_far.at[rows_of(spot), :],
            self.back_send.at[place.near + turn], self.back_recv.at[place.near + turn],
            place.partner,
        )

    def others(self, work):
        own = self.place.level * self.place.cell
        each(0, own, work)
        each(own + 1, self.place.near, work)

    def start(self):
        place = self.place

        @pl.when(place.stage == 0)
        def _():
            for copy in self.block_copies():
                copy.start()

        each(1, place.near, lambda distance: self.go_own(distance).start())
        self.recv[0:LANE_ROWS, :] = self.send_own[rows_of(place.spot), :]

        @pl.when(place.stage > 0)
        def _():
            for copy in self.block_copies():
                copy.start()

    def relay(self, stage):
        place = self.place

        @pl.when(place.stage == stage)
        def _():
            for copy in self.block_copies():
                copy.wait_recv()
            self.slots(self.far_block, self.far_meta, self.send_far)
            self.others(lambda turn: self.go_far(turn).start())
            slot = (place.near + stage * place.cell) * LANE_ROWS
            self.recv[slot:slot + LANE_ROWS, :] = self.send_far[rows_of(place.spot), :]

    def common(self):
        for load in self.loads[:3]:
            load.wait()
        gate = mm(self.normed[...], self.sg[...])
        hidden = (gate * jax.nn.sigmoid(gate) * mm(self.normed[...], self.su[...])).astype(BF16)
        step = self.width // 4
        for at in range(0, self.width, step):
            self.total[:, at:at + step] = mm(hidden, self.sd[:, at:at + step])
        for load in self.loads[3:]:
            load.wait()

    def serve(self, first, sources):
        main_rows, tail_rows = sources * LANE_ROWS, sources * self.tail
        low, width, base, piece = first * LANE_ROWS, self.width, self.base, self.piece
        start = self.groups * main_rows
        rows = start + tail_rows
        recv, ysend, xc, hc, yc = self.recv, self.ysend, self.xc, self.hc, self.yc

        def select(part, transposed):
            shape = (main_rows, tail_rows) if transposed else (tail_rows, main_rows)
            axis = 1 if transposed else 0
            return as_weight(iota(shape, 1 - axis) == iota(shape, axis) * self.parts + part)

        for group in range(self.groups):
            xc[group * main_rows:(group + 1) * main_rows, :] = recv[
                low:low + main_rows, group * width:(group + 1) * width
            ]
        for part in range(self.parts):
            xc[start:rows, part * piece:(part + 1) * piece] = mm(
                select(part, False), recv[low:low + main_rows, base:base + piece]
            ).astype(BF16)

        @pl.loop(0, hc.shape[1] // 256)
        def _(turn):
            columns = pl.ds(pl.multiple_of(turn * 256, 256), 256)
            gate = mm(xc[:rows, :], self.wg[:, columns])
            up = mm(xc[:rows, :], self.wu[:, columns])
            hc[:rows, columns] = (gate * jax.nn.sigmoid(gate) * up).astype(BF16)

        @pl.loop(0, width // 256)
        def _(turn):
            columns = pl.ds(pl.multiple_of(turn * 256, 256), 256)
            yc[:rows, columns] = mm(hc[:rows, :], self.wd[:, columns]).astype(BF16)

        for group in range(self.groups):
            ysend[low:low + main_rows, group * width:(group + 1) * width] = yc[
                group * main_rows:(group + 1) * main_rows, :
            ]
        total = jnp.zeros((main_rows, piece), F32)
        for part in range(self.parts):
            total = total + mm(
                select(part, True), yc[start:rows, part * piece:(part + 1) * piece]
            )
        ysend[low:low + main_rows, base:base + piece] = total.astype(BF16)

    def serve_own(self):
        place = self.place
        each(1, place.near, lambda distance: self.go_own(distance).wait_recv())
        self.serve(0, place.near)
        each(1, place.near, lambda distance: self.back_own(distance).start())
        self.ret_own[rows_of(place.spot), :] = self.ysend[0:LANE_ROWS, :]

    def serve_far(self, stage):
        place = self.place
        low = jnp.where(place.stage == stage, 1, 0)
        each(low, place.cell, lambda step: self.got_far(stage, step).wait_recv())
        first = place.near + stage * place.cell
        self.serve(first, place.cell)
        each(low, place.cell, lambda step: self.back_far(stage, step).start())

        @pl.when(place.stage == stage)
        def _():
            self.ret_far[rows_of(place.spot), :] = self.ysend[
                first * LANE_ROWS:(first + 1) * LANE_ROWS, :
            ]

    def mix(self, meta, ret, wait, store):
        turned = jnp.transpose(meta[...])[:self.tokens, :]
        whole = turned.astype(jnp.int32)
        mains, tails = self.keys(*[whole[:, row:row + 1] for row in range(4)])
        slot_lanes = iota((self.tokens, self.place.near * LANE_ROWS), 1)

        def mixing(first, second):
            values = jnp.where(slot_lanes == first, turned[:, 4:5], 0.0) + jnp.where(
                slot_lanes == second, turned[:, 5:6], 0.0
            )
            return halves(values)

        main_mix = [mixing(first, second) for first, second in mains]
        wait()
        for part in range(self.parts):
            low, high = part * self.piece, (part + 1) * self.piece
            total = jnp.zeros((self.tokens, self.piece), F32)
            for group, (coarse, fine) in enumerate(main_mix):
                values = ret[:, group * self.width + low:group * self.width + high]
                total = total + (mm(coarse, values) + mm(fine, values))
            coarse, fine = mixing(tails[0] + part, tails[1] + part)
            values = ret[:, self.base:self.base + self.piece]
            store(low, high, total + (mm(coarse, values) + mm(fine, values)))

    def mix_own(self):
        place = self.place

        def wait():
            each(1, place.near, lambda distance: self.back_own(distance).wait_recv())

        def store(low, high, value):
            self.total[:, low:high] = self.total[:, low:high] + value

        self.mix(self.meta, self.ret_own, wait, store)

    def mix_far(self, stage):
        @pl.when(self.place.stage == stage)
        def _():
            copies = self.back_copies()
            step = self.width // PIECES

            def wait():
                self.others(lambda turn: self.returned_far(turn).wait_recv())

            def store(low, high, value):
                self.far_out[:, low:high] = value.astype(BF16)
                if high % step == 0:
                    copies[high // step - 1].start()

            self.mix(self.far_meta, self.ret_far, wait, store)

    def close(self):
        step = self.width // PIECES
        for number, copy in enumerate(self.back_copies()):
            copy.wait_recv()
            columns = slice(number * step, (number + 1) * step)
            self.out_ref[:, columns] = (
                self.total[:, columns] + self.far_in[:, columns].astype(F32)
            ).astype(BF16)
        place = self.place
        each(1, place.near, lambda distance: self.go_own(distance).wait_send())
        each(1, place.near, lambda distance: self.back_own(distance).wait_send())
        self.others(lambda turn: self.go_far(turn).wait_send())
        for stage in range(place.depth):
            low = jnp.where(place.stage == stage, 1, 0)
            each(low, place.cell, lambda step: self.back_far(stage, step).wait_send())
        for copy in self.block_copies() + self.back_copies():
            copy.wait_send()


STATE_ROWS = 8


def nt(left, right, precision=None):
    return lax.dot_general(
        left, right, (((1,), (1,)), ((), ())), precision=precision, preferred_element_type=F32
    )


def halves(value):
    high = value.astype(BF16)
    return high, (value - high.astype(F32)).astype(BF16)


def log_one_plus(small):
    series = small * (1.0 - small * (0.5 - small * (1.0 / 3.0 - small * 0.25)))
    return jnp.where(small < 0.01, series, jnp.log(1.0 + small))


def mixer_parts(place_at, ep_count, tp_count, refs):
    (q_ref, k_ref, v_ref, in_ref, forget_ref, bias_ref, extra_ref, gate_ref, gain_ref, wo_hbm,
     out_ref, wo, locals_ref, state_send, state_recv, total_send, total_recv, total_ref,
     total_max, incoming, incoming_max, u_ref, squares_ref,
     u_recv, squares_recv, wo_sem, st_send, st_recv, tot_send, tot_recv, us_send, us_recv, sq_send, sq_recv) = refs
    exact = lax.Precision.HIGHEST
    heads, length = in_ref.shape
    blocks = length // BLK
    key_dim = q_ref.shape[1] // heads
    value_dim = v_ref.shape[1] // heads
    own_width = heads * value_dim
    scale = key_dim ** (-0.5)
    message = key_dim + STATE_ROWS
    share = length // tp_count
    share_blocks = share // BLK
    ep_at, tp_at = place_at.ep_at, place_at.tp_at
    load = pltpu.make_async_copy(wo_hbm, wo, wo_sem)

    def block_rows(ref, transform=lambda value, head: value):
        whole = ref[...]
        return jnp.concatenate(
            [
                transform(whole[head:head + 1, at * BLK:(at + 1) * BLK], head)
                for head in range(heads)
                for at in range(blocks)
            ],
            axis=0,
        )

    def key_block(head, at):
        return k_ref[at * BLK:(at + 1) * BLK, head * key_dim:(head + 1) * key_dim]

    def wide_values(head, at):
        values = v_ref[at * BLK:(at + 1) * BLK, head * value_dim:(head + 1) * value_dim]
        return jnp.concatenate([values, jnp.ones((BLK, value_dim), BF16)], axis=1)

    found = {}

    def grow(state, number):
        memory, top = state
        total = found["total"][number:number + 1, :]
        block_top = found["block_top"][number:number + 1, :]
        new_top = jnp.maximum(top + total, block_top)
        memory = jnp.exp(top + total - new_top) * memory + jnp.exp(
            block_top - new_top
        ) * locals_ref[number]
        return memory, new_top

    def diagonal():
        shape = (key_dim, value_dim)
        return iota(shape, 0) == iota(shape, 1)

    def early():
        load.start()
        logits = block_rows(forget_ref, lambda value, head: value + bias_ref[:, head:head + 1])
        kept = jnp.minimum(logits, 0.0) - log_one_plus(jnp.exp(-jnp.abs(logits)))
        kept = kept + block_rows(extra_ref)
        gates = block_rows(in_ref)
        upper = (iota((BLK, BLK), 0) <= iota((BLK, BLK), 1)).astype(F32)
        cumulative = jnp.dot(kept, upper, precision=exact, preferred_element_type=F32)
        total = cumulative[:, BLK - 1:BLK]
        gap = total - cumulative + gates
        block_top = jnp.max(gap, axis=1, keepdims=True)
        weight = jnp.exp(gap - block_top)
        found["total"], found["block_top"] = total, block_top
        found["cumulative"], found["shift"] = cumulative, gates - cumulative
        eye = (iota((key_dim, key_dim), 0) == iota((key_dim, key_dim), 1)).astype(F32).astype(BF16)
        for head in range(heads):
            state = (
                jnp.zeros((key_dim, 2 * value_dim), F32), jnp.full((1, 1), -1e30, F32)
            )
            decay = jnp.zeros((1, 1), F32)
            for at in range(blocks):
                number = head * blocks + at
                turned = nt(eye, key_block(head, at)) * weight[number:number + 1, :]
                high, low = halves(turned)
                values = wide_values(head, at)
                locals_ref[number] = mm(high, values) + mm(low, values)
                state = grow(state, number)
                decay = decay + total[number:number + 1, :]
            memory, top = state
            low_row = head * message
            state_send[low_row:low_row + key_dim, :] = memory[:, :value_dim]
            norm = jnp.sum(
                jnp.where(diagonal(), memory[:, value_dim:], 0.0), axis=0, keepdims=True
            )
            row = iota((STATE_ROWS, value_dim), 0)
            state_send[low_row + key_dim:low_row + message, :] = jnp.where(
                row == 0, norm, jnp.where(row == 1, top, decay)
            )

    span = place_at.depth * place_at.side
    own_at = lax.rem(ep_at, span)
    lower_half = place_at.half == 0

    def state_copy(distance, sign):
        at = lax.rem(own_at + sign * distance + span, span)
        return remote(
            state_send, state_recv.at[distance], st_send.at[distance], st_recv.at[distance],
            (place_at.half * span + at, tp_at),
        )

    def total_copy():
        return remote(total_send, total_recv, tot_send, tot_recv, place_at.partner)

    def sends_to(distance):
        return lower_half | (own_at + distance < span)

    def takes_from(distance):
        return lower_half | (own_at >= distance)

    def u_copies(target, sender):
        place = pl.ds(pl.multiple_of(sender * own_width, own_width), own_width)
        return [
            remote(
                u_ref.at[target * share:(target + 1) * share, :], u_recv.at[:, place],
                us_send.at[target], us_recv.at[sender], (ep_at, target),
            ),
            remote(
                squares_ref.at[target], squares_recv.at[sender],
                sq_send.at[target], sq_recv.at[sender], (ep_at, target),
            ),
        ]

    def send_states():
        for distance in range(1, span):
            @pl.when(sends_to(distance))
            def _():
                state_copy(distance, 1).start()

    def absorb(memory_ref, max_ref, message_ref):
        for head in range(heads):
            low_row = head * message
            memory = message_ref[low_row:low_row + key_dim, :]
            extra = message_ref[low_row + key_dim:low_row + message, :]
            norm = jnp.sum(jnp.where(diagonal(), extra[0:1, :], 0.0), axis=1, keepdims=True)
            top, decay = extra[1:2, :], extra[2:3, :]
            old_top = max_ref[head, 0:1, :]
            new_top = jnp.maximum(old_top + decay, top)
            left = jnp.exp(old_top + decay - new_top)
            right = jnp.exp(top - new_top)
            memory_ref[head, :, :value_dim] = (
                left * memory_ref[head, :, :value_dim] + right * memory
            )
            memory_ref[head, :, value_dim:] = (
                left * memory_ref[head, :, value_dim:] + right * norm
            )
            max_ref[head] = jnp.broadcast_to(new_top, max_ref.shape[1:])

    def take_states():
        for distance in range(1, span):
            @pl.when(takes_from(distance))
            def _():
                state_copy(distance, 1).wait_recv()

        @pl.when(lower_half)
        def _():
            total_ref[...] = jnp.zeros_like(total_ref)
            total_max[...] = jnp.full_like(total_max, -1e30)
            for distance in range(span - 1, 0, -1):
                @pl.when(own_at >= distance)
                def _():
                    absorb(total_ref, total_max, state_recv.at[distance])
            incoming[...] = total_ref[...]
            incoming_max[...] = total_max[...]
            absorb(total_ref, total_max, state_send)
            for distance in range(span - 1, 0, -1):
                @pl.when(own_at < distance)
                def _():
                    absorb(total_ref, total_max, state_recv.at[distance])
            for head in range(heads):
                low_row = head * message
                total_send[low_row:low_row + key_dim, :] = total_ref[head, :, :value_dim]
                norm = jnp.sum(
                    jnp.where(diagonal(), total_ref[head, :, value_dim:], 0.0),
                    axis=0, keepdims=True,
                )
                row = iota((STATE_ROWS, value_dim), 0)
                total_send[low_row + key_dim:low_row + message, :] = jnp.where(
                    row == 0, norm, jnp.where(row == 1, total_max[head], 0.0)
                )
            total_copy().start()

    def take_total():
        @pl.when(jnp.logical_not(lower_half))
        def _():
            incoming[...] = jnp.zeros_like(incoming)
            incoming_max[...] = jnp.full_like(incoming_max, -1e30)
            total_copy().wait_recv()
            absorb(incoming, incoming_max, total_recv)
            for distance in range(span - 1, 0, -1):
                @pl.when(own_at >= distance)
                def _():
                    absorb(incoming, incoming_max, state_recv.at[distance])

    def walk(low_block, high_block):
        if low_block == 0:
            found["states"] = [
                (incoming[head], incoming_max[head, 0:1, 0:1]) for head in range(heads)
            ]
            found["columns"] = jnp.transpose(found["cumulative"])
        states, columns = found["states"], found["columns"]
        lower = iota((BLK, BLK), 0) >= iota((BLK, BLK), 1)
        ones = jnp.ones((STATE_ROWS, value_dim), F32)
        for at in range(low_block, high_block):
            squares = jnp.zeros((STATE_ROWS, BLK), F32)
            for head in range(heads):
                number = head * blocks + at
                memory, top = states[head]
                query = q_ref[at * BLK:(at + 1) * BLK, head * key_dim:(head + 1) * key_dim]
                column = columns[:, number:number + 1]
                gap = jnp.where(
                    lower, column + found["shift"][number:number + 1, :], -jnp.inf
                )
                carried = column + top
                stabilizer = jnp.maximum(carried, jnp.max(gap, axis=1, keepdims=True))
                scores = nt(query, key_block(head, at)) * scale * jnp.exp(gap - stabilizer)
                high, low = halves(scores)
                values = wide_values(head, at)
                sums = mm(high, values) + mm(low, values)
                high, low = halves(memory)
                sums = sums + (jnp.exp(carried - stabilizer) * scale) * (
                    mm(query, high) + mm(query, low)
                )
                hidden = sums[:, :value_dim] / jnp.maximum(
                    jnp.abs(sums[:, value_dim:]), jnp.exp(-stabilizer)
                )
                squares = squares + nt(ones, hidden * hidden, exact)
                place = slice(head * value_dim, (head + 1) * value_dim)
                gate = gate_ref[at * BLK:(at + 1) * BLK, place].astype(F32)
                u_ref[at * BLK:(at + 1) * BLK, place] = (
                    hidden * gain_ref[:, place] * jax.nn.sigmoid(gate)
                ).astype(BF16)
                states[head] = grow(states[head], number)
            squares_ref[at // share_blocks, at % share_blocks] = squares
            if at % share_blocks == share_blocks - 1:
                target = at // share_blocks

                @pl.when(tp_at != target)
                def _():
                    for copy in u_copies(target, tp_at):
                        copy.start()

                @pl.when(tp_at == target)
                def _():
                    place = pl.ds(pl.multiple_of(tp_at * own_width, own_width), own_width)
                    u_recv[:, place] = u_ref[target * share:(target + 1) * share, :]
                    squares_recv[tp_at] = squares_ref[target]

    def late():
        for sender in range(tp_count):
            @pl.when(tp_at != sender)
            def _():
                for copy in u_copies(0, sender):
                    copy.wait_recv()
        squares = squares_recv[0]
        for sender in range(1, tp_count):
            squares = squares + squares_recv[sender]
        inverse_row = lax.rsqrt(squares / (heads * tp_count * value_dim) + 1e-6)
        eye = (iota((BLK, BLK), 0) == iota((BLK, BLK), 1)).astype(F32)
        load.wait()
        width = wo.shape[1]
        for at in range(share_blocks):
            inverse = nt(eye, inverse_row[at], exact)[:, 0:1]

            @pl.loop(0, width // 512)
            def _(turn):
                place = pl.ds(pl.multiple_of(turn * 512, 512), 512)
                product = mm(u_recv[at * BLK:(at + 1) * BLK, :], wo[:, place])
                out_ref[at * BLK:(at + 1) * BLK, place] = (product * inverse).astype(BF16)


    def close():
        for distance in range(1, span):
            @pl.when(sends_to(distance))
            def _():
                state_copy(distance, 1).wait_send()

        @pl.when(lower_half)
        def _():
            total_copy().wait_send()

        for target in range(tp_count):
            @pl.when(tp_at != target)
            def _():
                for copy in u_copies(target, tp_at):
                    copy.wait_send()

    return early, send_states, take_states, take_total, walk, late, close


def on_device(
    queries,
    head_key_rows,
    head_value_rows,
    log_input_gate,
    forget_logits,
    head_forget_bias,
    extra_log_forget,
    output_gate_logits,
    head_norm_gain,
    mixer_output_weight,
    second_batch_input,
    expert_norm_gain,
    routed_expert_index,
    routed_copy_weight,
    routed_gate_weight,
    routed_up_weight,
    routed_down_weight,
    shared_gate_weight,
    shared_up_weight,
    shared_down_weight,
):
    tokens, width = second_batch_input.shape
    ep_count = lax.axis_size("ep")
    tp_count = lax.axis_size("tp")
    count = ep_count * tp_count
    top_count = routed_expert_index.shape[1]
    capacity = max(2, 3 * tokens * top_count // (2 * count))
    wire = capacity * width // LANE_ROWS
    side = max(1, tp_count // CORES)
    near = count // 2
    span = ep_count // 2
    rows = near * capacity
    padded = -(-tokens // 128) * 128
    hidden_width = routed_gate_weight.shape[2]
    length = queries.shape[0]
    heads = head_forget_bias.shape[0]
    key_dim = queries.shape[1] // heads
    value_dim = head_value_rows.shape[1] // heads
    blocks = length // BLK
    share = length // tp_count
    dma = pltpu.SemaphoreType.DMA
    vmem = pl.BlockSpec(memory_space=pltpu.VMEM)
    hbm = pl.BlockSpec(memory_space=pl.ANY)

    block = pltpu.VMEM((tokens, width), BF16)
    meta = pltpu.VMEM((STATE_ROWS, padded), F32)
    half_slots = pltpu.VMEM((near * LANE_ROWS, wire), BF16)
    slots = pltpu.VMEM((2 * near * LANE_ROWS, wire), BF16)
    moe_scratch = (
        [block, meta, block, meta]
        + [half_slots, half_slots, slots, slots, half_slots, half_slots]
        + [block, block]
        + [
            pltpu.VMEM(array.shape[-2:], BF16)
            for array in (
                routed_gate_weight, routed_up_weight, routed_down_weight,
                shared_gate_weight, shared_up_weight, shared_down_weight,
            )
        ]
        + [
            pltpu.VMEM((rows, width), BF16),
            pltpu.VMEM((rows, hidden_width), BF16),
            pltpu.VMEM((rows, width), BF16),
            pltpu.VMEM((tokens, width), F32),
            dma((6,)), dma((count,)), dma((count,)), dma((count,)), dma((count,)),
            dma((2 * PIECES + 1,)), dma((2 * PIECES + 1,)),
        ]
    )
    message = heads * (key_dim + STATE_ROWS)
    mixer_scratch = [
        pltpu.VMEM(mixer_output_weight.shape, BF16),
        pltpu.VMEM((heads * blocks, key_dim, 2 * value_dim), F32),
        pltpu.VMEM((message, value_dim), F32),
        pltpu.VMEM((span, message, value_dim), F32),
        pltpu.VMEM((message, value_dim), F32),
        pltpu.VMEM((message, value_dim), F32),
        pltpu.VMEM((heads, key_dim, 2 * value_dim), F32),
        pltpu.VMEM((heads, STATE_ROWS, value_dim), F32),
        pltpu.VMEM((heads, key_dim, 2 * value_dim), F32),
        pltpu.VMEM((heads, STATE_ROWS, value_dim), F32),
        pltpu.VMEM((length, heads * value_dim), BF16),
        pltpu.VMEM((tp_count, share // BLK, STATE_ROWS, BLK), F32),
        pltpu.VMEM((share, tp_count * heads * value_dim), BF16),
        pltpu.VMEM((tp_count, share // BLK, STATE_ROWS, BLK), F32),
        dma, dma((span,)), dma((span,)), dma, dma,
        dma((tp_count,)), dma((tp_count,)), dma((tp_count,)), dma((tp_count,)),
    ]

    def kernel(*refs):
        mixer_in, moe_in = refs[:10], refs[10:20]
        mixer_out, moe_out = refs[20], refs[21]
        scratch = refs[22:]
        cut = len(moe_scratch)
        place = Place(ep_count, tp_count)
        early, send_states, take_states, take_total, walk, late, close = mixer_parts(
            place, ep_count, tp_count, (*mixer_in, mixer_out, *scratch[cut:])
        )
        experts = Experts(place, capacity, (*moe_in, moe_out, *scratch[:cut]))
        depth = place.depth
        experts.open()
        experts.start()
        early()
        send_states()
        experts.common()
        experts.relay(0)
        experts.serve_own()
        take_states()
        for stage in range(depth):
            experts.serve_far(stage)
            if stage + 1 < depth:
                experts.relay(stage + 1)
            if stage == 0:
                take_total()
            walk(blocks * stage // depth, blocks * (stage + 1) // depth)
            if stage == 0:
                experts.mix_own()
            experts.mix_far(stage)
        late()
        experts.close()
        close()

    return pl.pallas_call(
        kernel,
        out_shape=(
            jax.ShapeDtypeStruct((share, width), BF16),
            jax.ShapeDtypeStruct((tokens, width), BF16),
        ),
        in_specs=[vmem] * 9 + [hbm] + [vmem] * 4 + [hbm] * 6,
        out_specs=(vmem, vmem),
        scratch_shapes=moe_scratch + mixer_scratch,
        compiler_params=pltpu.CompilerParams(
            collective_id=0, has_side_effects=True, vmem_limit_bytes=62 * 1024 * 1024
        ),
        name="both",
    )(
        queries, head_key_rows, head_value_rows, log_input_gate.T, forget_logits.T,
        head_forget_bias[None, :], extra_log_forget.T, output_gate_logits,
        head_norm_gain[None, :], mixer_output_weight,
        second_batch_input, expert_norm_gain[None, :], routed_expert_index.T,
        routed_copy_weight.T, routed_gate_weight, routed_up_weight,
        routed_down_weight, shared_gate_weight, shared_up_weight, shared_down_weight,
    )


def solution(mesh):
    in_specs = (
        P("ep", "tp"),
        P("ep", "tp"),
        P("ep", "tp"),
        P("ep", "tp"),
        P("ep", "tp"),
        P("tp"),
        P("ep", "tp"),
        P("ep", "tp"),
        P("tp"),
        P(),
        P(("ep", "tp"), None),
        P(),
        P(("ep", "tp"), None),
        P(("ep", "tp"), None),
        P(("ep", "tp"), None, None),
        P(("ep", "tp"), None, None),
        P(("ep", "tp"), None, None),
        P(),
        P(),
        P(),
    )
    out_specs = (P(("ep", "tp"), None), P(("ep", "tp"), None))
    return jax.shard_map(
        on_device, mesh=mesh, in_specs=in_specs, out_specs=out_specs, check_vma=False
    )
```

time: 168 us -> 140 us (0.83)
  Pallas kernels: 159 us -> 135 us
  local copies, waits for them, and re-layouts: 8.6 us -> 4.39 us
    pallas_call x1, Pallas kernels: 159 us -> 135 us  [on_device(): pl.pallas_call(kernel, out_shape=(jax.ShapeDtypeStruct((share, width), BF...]
    unnamed x4 -> x2, local copies, waits for them, and re-layouts: 7.28 us -> 4.39 us
where the time goes in v1:
time: 140 us
  Pallas kernels  135 us (96%)
  local copies, waits for them, and re-layouts  4.39 us (3%)
    pallas_call x1, Pallas kernels, on_device(): pl.pallas_call(kernel, out_shape=(jax.ShapeDtypeStruct((share, width), BF...  135 us
    unnamed x2, local copies, waits for them, and re-layouts  4.39 us

profile of v1, /device:TPU:0, one launch (start us, length us, event | category | flops | bytes accessed | tf_op | source)
XLA Modules:
  0.0 139.9 jit_solution(5775451651075584532)
XLA Ops:
  0.6 134.9 %both.1 = (bf16[256,2048]{1,0:T(8,128)(2,1)}, bf16[192,2048]{1,0:T(8,128)(2,1)}) custom-call(bf16[1024,128]{1,0:T(8,128)(2,1)} %refs_0_.1, bf16[1024,128]{1,0:T(8,128)(2,1)} %refs_1_.1, bf16[1024,256]{1,0:T(8,128)(2,1)} %refs_2_.1, f32[2,1024]{1,0:T(2,128)} %bitcast.8, f32[2,1024]{1,0:T(2,128)} %bitcast.9, f32[1,2]{1,0:T(1,128)} %bitcast.15, ...), custom_call_target="tpu_custom_call" | custom-call | tf_op jit(solution)/shard_map/both/pallas_call | solution.py:867
  135.5 2.3 %copy.24 = bf16[256,2048]{1,0:T(8,128)(2,1)} copy(bf16[256,2048]{1,0:T(8,128)(2,1)} %get-tuple-element.4) | data formatting | bytes 2097152
  137.8 2.1 %copy.25 = bf16[192,2048]{1,0:T(8,128)(2,1)} copy(bf16[192,2048]{1,0:T(8,128)(2,1)} %get-tuple-element.5) | data formatting | bytes 1572864

commit v2 on v1

--- a/solution.py
+++ b/solution.py
@@ -39,7 +39,9 @@
         self.level = plane - self.half * self.depth
         self.stage = self.half * self.level + (1 - self.half) * (self.depth - 1 - self.level)
         self.spot = self.level * self.cell + self.row * tp_count + self.tp_at
-        self.partner = ((self.planes - 1 - plane) * self.side + self.row, self.tp_at)
+        self.inner = self.stage == 0
+        self.low = jnp.where(self.inner, 1, 0)
+        self.proxy = self.beyond(0)
 
     def at(self, level, row, tp):
         device = ((self.half * self.depth + level) * self.side + row, tp)
@@ -56,8 +58,9 @@
         level = lax.rem(self.level + sign * level_step + self.depth, self.depth)
         return self.at(level, *self.across(lax.rem(distance, self.cell), sign))
 
-    def level_of(self, stage):
-        return self.half * stage + (1 - self.half) * (self.depth - 1 - stage)
+    def beyond(self, stage):
+        plane = (1 - self.half) * (self.depth + stage) + self.half * (self.depth - 1 - stage)
+        return plane * self.side + self.row, self.tp_at
 
 
 def each(low, high, work):
@@ -89,15 +92,18 @@
          su_hbm, sd_hbm, self.out_ref, self.normed, self.meta, self.far_block, self.far_meta,
          self.send_own, self.send_far, self.recv, self.ysend, self.ret_own, self.ret_far,
          self.far_out, self.far_in, self.wg, self.wu, self.wd, self.sg, self.su, self.sd, self.xc,
-         self.hc, self.yc, self.total, load_sem, self.go_send, self.go_recv, self.back_send,
-         self.back_recv, self.over_send, self.over_recv) = refs
+         self.hc, self.yc, self.total, load_sem, self.go_send, self.go_recv, self.far_send,
+         self.back_send, self.back_recv, self.far_recv, self.over_send, self.over_recv,
+         self.result_send, self.result_recv, self.meta_send, self.meta_recv) = refs
         self.place = place
         self.tokens, self.width = self.x_ref.shape
+        self.step = self.width // PIECES
         self.groups = capacity // LANE_ROWS
         self.tail = capacity - self.groups * LANE_ROWS
         self.parts = LANE_ROWS // self.tail
-        self.piece = self.width // self.parts
-        self.base = self.groups * self.width
+        self.piece = self.step // self.parts
+        self.base = self.groups * self.step
+        self.wire = self.base + self.piece
         self.loads = [
             pltpu.make_async_copy(source, target, load_sem.at[number])
             for number, (source, target) in enumerate(
@@ -118,7 +124,12 @@
             )
 
         each(1, place.near, lambda distance: greet(place.away(distance, 1)[0]))
-        greet(place.partner)
+        greet(place.proxy)
+
+        @pl.when(place.inner)
+        def _():
+            for stage in range(1, place.depth):
+                greet(place.beyond(stage))
 
         floats = self.x_ref[...].astype(F32)
         inverse = lax.rsqrt(jnp.mean(floats * floats, axis=1, keepdims=True) + 1e-6)
@@ -139,8 +150,14 @@
             jnp.where(hit_second, earlier, 0.0), axis=0, keepdims=True
         )
         self.meta[4:6, :tokens] = self.weight_ref[...]
-        self.slots(self.normed, self.meta, self.send_own)
-        pl.semaphore_wait(barrier, place.near)
+        for piece in range(PIECES):
+            self.slots(piece, self.normed, self.meta, self.send_own)
+
+    def meet(self):
+        place = self.place
+        pl.semaphore_wait(
+            pltpu.get_barrier_semaphore(), place.near - 1 + jnp.where(place.inner, place.depth, 1)
+        )
 
     def keys(self, first, second, place_first, place_second):
         near, low = self.place.near, self.place.half * self.place.near
@@ -162,95 +179,128 @@
         ]
         return mains, (tail(first, place_first), tail(second, place_second))
 
-    def slots(self, block, meta, send):
+    def slots(self, piece, block, meta, send):
         whole = meta[:, :self.tokens].astype(jnp.int32)
         mains, tails = self.keys(*[whole[row:row + 1, :] for row in range(4)])
         slot_rows = iota((self.place.near * LANE_ROWS, self.tokens), 0)
-        step = self.width // 4
+        low, to = piece * self.step, piece * self.wire
+        step = self.step // 2
         for group, (first, second) in enumerate(mains):
             pick = as_weight((slot_rows == first) | (slot_rows == second))
-            for at in range(0, self.width, step):
-                send[:, group * self.width + at:group * self.width + at + step] = mm(
-                    pick, block[:, at:at + step]
+            for at in range(0, self.step, step):
+                start = to + group * self.step + at
+                send[:, start:start + step] = mm(
+                    pick, block[:, low + at:low + at + step]
                 ).astype(BF16)
         total = jnp.zeros((self.place.near * LANE_ROWS, self.piece), F32)
         for part in range(self.parts):
             pick = as_weight((slot_rows == tails[0] + part) | (slot_rows == tails[1] + part))
-            total = total + mm(pick, block[:, part * self.piece:(part + 1) * self.piece])
-        send[:, self.base:self.base + self.piece] = total.astype(BF16)
-
-    def over(self, source, target, first):
-        step = self.width // PIECES
-        return [
-            remote(
-                source.at[:, number * step:(number + 1) * step],
-                target.at[:, number * step:(number + 1) * step],
-                self.over_send.at[first + number], self.over_recv.at[first + number],
-                self.place.partner,
-            )
-            for number in range(PIECES)
-        ]
-
-    def block_copies(self):
-        return [
-            remote(
-                self.meta, self.far_meta, self.over_send.at[2 * PIECES],
-                self.over_recv.at[2 * PIECES], self.place.partner,
-            )
-        ] + self.over(self.normed, self.far_block, 0)
-
-    def back_copies(self):
-        return self.over(self.far_out, self.far_in, PIECES)
-
-    def go_own(self, distance):
+            at = low + part * self.piece
+            total = total + mm(pick, block[:, at:at + self.piece])
+        send[:, to + self.base:to + self.wire] = total.astype(BF16)
+
+    def columns(self, piece):
+        return slice(piece * self.step, (piece + 1) * self.step)
+
+    def wires(self, piece):
+        return slice(piece * self.wire, (piece + 1) * self.wire)
+
+    def meta_copy(self):
+        return remote(
+            self.meta, self.far_meta.at[self.place.stage], self.meta_send,
+            self.meta_recv.at[self.place.stage], self.place.proxy,
+        )
+
+    def meta_from(self, stage):
+        return remote(
+            self.meta, self.far_meta.at[stage], self.meta_send, self.meta_recv.at[stage],
+            self.place.proxy,
+        )
+
+    def block_to(self, stage, piece):
+        columns = self.columns(piece)
+        return remote(
+            self.normed.at[:, columns], self.far_block.at[stage, :, columns],
+            self.over_send.at[piece], self.over_recv.at[stage, piece], self.place.proxy,
+        )
+
+    def result_to(self, stage, piece):
+        columns = self.columns(piece)
+        return remote(
+            self.far_out.at[stage, :, columns], self.far_in.at[:, columns],
+            self.result_send.at[stage, piece], self.result_recv.at[piece],
+            self.place.beyond(stage),
+        )
+
+    def go_own(self, distance, piece):
         device, spot = self.place.away(distance, 1)
-        return remote(
-            self.send_own.at[rows_of(spot), :], self.recv.at[rows_of(distance), :],
-            self.go_send.at[distance], self.go_recv.at[distance], device,
-        )
-
-    def back_own(self, distance):
+        wires = self.wires(piece)
+        return remote(
+            self.send_own.at[rows_of(spot), wires], self.recv.at[rows_of(distance), wires],
+            self.go_send.at[piece, distance], self.go_recv.at[piece, distance], device,
+        )
+
+    def back_own(self, distance, piece):
         device, _ = self.place.away(distance, -1)
-        return remote(
-            self.ysend.at[rows_of(distance), :], self.ret_own.at[rows_of(self.place.spot), :],
-            self.back_send.at[distance], self.back_recv.at[distance], device,
-        )
-
-    def go_far(self, turn):
+        wires = self.wires(piece)
+        return remote(
+            self.ysend.at[rows_of(distance), wires],
+            self.ret_own.at[rows_of(self.place.spot), wires],
+            self.back_send.at[piece, distance], self.back_recv.at[piece, distance], device,
+        )
+
+    def back_here(self, distance, piece):
+        _, spot = self.place.away(distance, 1)
+        wires = self.wires(piece)
+        return remote(
+            self.ysend.at[rows_of(distance), wires], self.ret_own.at[rows_of(spot), wires],
+            self.back_send.at[piece, distance], self.back_recv.at[piece, distance],
+            self.place.proxy,
+        )
+
+    def go_far(self, stage, turn, piece):
         place = self.place
         level, step = turn // place.cell, lax.rem(turn, place.cell)
         device, spot = place.at(level, *place.across(step, 1))
-        slot = place.near + place.stage * place.cell + step
-        return remote(
-            self.send_far.at[rows_of(spot), :], self.recv.at[rows_of(slot), :],
-            self.go_send.at[place.near + turn], self.go_recv.at[slot], device,
-        )
-
-    def got_far(self, stage, step):
+        slot = place.near + stage * place.cell + step
+        wires = self.wires(piece)
+        return remote(
+            self.send_far.at[stage, rows_of(spot), wires], self.recv.at[rows_of(slot), wires],
+            self.far_send.at[piece, stage * place.near + turn], self.go_recv.at[piece, slot],
+            device,
+        )
+
+    def got_far(self, stage, step, piece):
         slot = self.place.near + stage * self.place.cell + step
-        return remote(
-            self.send_far.at[rows_of(0), :], self.recv.at[rows_of(slot), :],
-            self.go_send.at[slot], self.go_recv.at[slot], self.place.partner,
-        )
-
-    def back_far(self, stage, step):
+        wires = self.wires(piece)
+        return remote(
+            self.send_far.at[stage, rows_of(0), wires], self.recv.at[rows_of(slot), wires],
+            self.far_send.at[piece, 0], self.go_recv.at[piece, slot], self.place.proxy,
+        )
+
+    def back_far(self, stage, step, piece):
         place = self.place
-        device, _ = place.at(place.level_of(stage), *place.across(step, -1))
+        level = (1 - place.half) * (place.depth - 1)
+        device, _ = place.at(level, *place.across(step, -1))
         slot = place.near + stage * place.cell + step
-        return remote(
-            self.ysend.at[rows_of(slot), :], self.ret_far.at[rows_of(place.spot), :],
-            self.back_send.at[slot],
-            self.back_recv.at[place.near + place.level * place.cell + step], device,
-        )
-
-    def returned_far(self, turn):
+        wires = self.wires(piece)
+        return remote(
+            self.ysend.at[rows_of(slot), wires],
+            self.ret_far.at[stage, rows_of(place.spot), wires],
+            self.back_send.at[piece, slot],
+            self.far_recv.at[piece, stage * place.near + place.level * place.cell + step],
+            device,
+        )
+
+    def returned_far(self, stage, turn, piece):
         place = self.place
         level, step = turn // place.cell, lax.rem(turn, place.cell)
         _, spot = place.at(level, *place.across(step, 1))
-        return remote(
-            self.ysend.at[rows_of(0), :], self.ret_far.at[rows_of(spot), :],
-            self.back_send.at[place.near + turn], self.back_recv.at[place.near + turn],
-            place.partner,
+        wires = self.wires(piece)
+        return remote(
+            self.ysend.at[rows_of(0), wires], self.ret_far.at[stage, rows_of(spot), wires],
+            self.back_send.at[piece, 0], self.far_recv.at[piece, stage * place.near + turn],
+            place.proxy,
         )
 
     def others(self, work):
@@ -261,30 +311,39 @@
     def start(self):
         place = self.place
 
-        @pl.when(place.stage == 0)
+        @pl.when(place.inner)
         def _():
-            for copy in self.block_copies():
-                copy.start()
-
-        each(1, place.near, lambda distance: self.go_own(distance).start())
+            self.meta_copy().start()
+            for piece in range(PIECES):
+                self.block_to(0, piece).start()
+
+        for piece in range(PIECES):
+            each(1, place.near, lambda distance: self.go_own(distance, piece).start())
         self.recv[0:LANE_ROWS, :] = self.send_own[rows_of(place.spot), :]
 
-        @pl.when(place.stage > 0)
+    def start_outer(self):
+        place = self.place
+
+        @pl.when(jnp.logical_not(place.inner))
         def _():
-            for copy in self.block_copies():
-                copy.start()
-
-    def relay(self, stage):
+            self.meta_copy().start()
+            for piece in range(PIECES):
+                self.block_to(place.stage, piece).start()
+
+    def relay(self, stage, piece):
         place = self.place
 
-        @pl.when(place.stage == stage)
+        @pl.when(place.inner)
         def _():
-            for copy in self.block_copies():
-                copy.wait_recv()
-            self.slots(self.far_block, self.far_meta, self.send_far)
-            self.others(lambda turn: self.go_far(turn).start())
+            if piece == 0:
+                self.meta_from(stage).wait_recv()
+            self.block_to(stage, piece).wait_recv()
+            self.slots(piece, self.far_block.at[stage], self.far_meta.at[stage], self.send_far.at[stage])
+            self.others(lambda turn: self.go_far(stage, turn, piece).start())
             slot = (place.near + stage * place.cell) * LANE_ROWS
-            self.recv[slot:slot + LANE_ROWS, :] = self.send_far[rows_of(place.spot), :]
+            self.recv[slot:slot + LANE_ROWS, self.wires(piece)] = self.send_far[
+                stage, rows_of(place.spot), self.wires(piece)
+            ]
 
     def common(self):
         for load in self.loads[:3]:
@@ -297,9 +356,9 @@
         for load in self.loads[3:]:
             load.wait()
 
-    def serve(self, first, sources):
+    def serve(self, first, sources, arrive, leave, between):
         main_rows, tail_rows = sources * LANE_ROWS, sources * self.tail
-        low, width, base, piece = first * LANE_ROWS, self.width, self.base, self.piece
+        low, piece = first * LANE_ROWS, self.piece
         start = self.groups * main_rows
         rows = start + tail_rows
         recv, ysend, xc, hc, yc = self.recv, self.ysend, self.xc, self.hc, self.yc
@@ -309,14 +368,18 @@
             axis = 1 if transposed else 0
             return as_weight(iota(shape, 1 - axis) == iota(shape, axis) * self.parts + part)
 
-        for group in range(self.groups):
-            xc[group * main_rows:(group + 1) * main_rows, :] = recv[
-                low:low + main_rows, group * width:(group + 1) * width
-            ]
-        for part in range(self.parts):
-            xc[start:rows, part * piece:(part + 1) * piece] = mm(
-                select(part, False), recv[low:low + main_rows, base:base + piece]
-            ).astype(BF16)
+        for number in range(PIECES):
+            arrive(number)
+            at, to = number * self.wire, number * self.step
+            for group in range(self.groups):
+                xc[group * main_rows:(group + 1) * main_rows, to:to + self.step] = recv[
+                    low:low + main_rows, at + group * self.step:at + (group + 1) * self.step
+                ]
+            for part in range(self.parts):
+                xc[start:rows, to + part * piece:to + (part + 1) * piece] = mm(
+                    select(part, False),
+                    recv[low:low + main_rows, at + self.base:at + self.wire],
+                ).astype(BF16)
 
         @pl.loop(0, hc.shape[1] // 256)
         def _(turn):
@@ -325,42 +388,64 @@
             up = mm(xc[:rows, :], self.wu[:, columns])
             hc[:rows, columns] = (gate * jax.nn.sigmoid(gate) * up).astype(BF16)
 
-        @pl.loop(0, width // 256)
-        def _(turn):
-            columns = pl.ds(pl.multiple_of(turn * 256, 256), 256)
-            yc[:rows, columns] = mm(hc[:rows, :], self.wd[:, columns]).astype(BF16)
-
-        for group in range(self.groups):
-            ysend[low:low + main_rows, group * width:(group + 1) * width] = yc[
-                group * main_rows:(group + 1) * main_rows, :
-            ]
-        total = jnp.zeros((main_rows, piece), F32)
-        for part in range(self.parts):
-            total = total + mm(
-                select(part, True), yc[start:rows, part * piece:(part + 1) * piece]
-            )
-        ysend[low:low + main_rows, base:base + piece] = total.astype(BF16)
+        between()
+        for number in range(PIECES):
+            at, to = number * self.wire, number * self.step
+
+            @pl.loop(0, self.step // 256)
+            def _(turn):
+                columns = pl.ds(pl.multiple_of(to + turn * 256, 256), 256)
+                yc[:rows, columns] = mm(hc[:rows, :], self.wd[:, columns]).astype(BF16)
+
+            for group in range(self.groups):
+                ysend[
+                    low:low + main_rows, at + group * self.step:at + (group + 1) * self.step
+                ] = yc[group * main_rows:(group + 1) * main_rows, to:to + self.step]
+            total = jnp.zeros((main_rows, piece), F32)
+            for part in range(self.parts):
+                total = total + mm(
+                    select(part, True),
+                    yc[start:rows, to + part * piece:to + (part + 1) * piece],
+                )
+            ysend[low:low + main_rows, at + self.base:at + self.wire] = total.astype(BF16)
+            leave(number)
 
     def serve_own(self):
         place = self.place
-        each(1, place.near, lambda distance: self.go_own(distance).wait_recv())
-        self.serve(0, place.near)
-        each(1, place.near, lambda distance: self.back_own(distance).start())
-        self.ret_own[rows_of(place.spot), :] = self.ysend[0:LANE_ROWS, :]
+
+        def arrive(piece):
+            with jax.named_scope("wait_own"):
+                each(1, place.near, lambda distance: self.go_own(distance, piece).wait_recv())
+
+        def leave(piece):
+            each(1, place.near, lambda distance: self.back_own(distance, piece).start())
+            self.ret_own[rows_of(place.spot), self.wires(piece)] = self.ysend[
+                0:LANE_ROWS, self.wires(piece)
+            ]
+
+        self.serve(0, place.near, arrive, leave, self.start_outer)
 
     def serve_far(self, stage):
         place = self.place
-        low = jnp.where(place.stage == stage, 1, 0)
-        each(low, place.cell, lambda step: self.got_far(stage, step).wait_recv())
         first = place.near + stage * place.cell
-        self.serve(first, place.cell)
-        each(low, place.cell, lambda step: self.back_far(stage, step).start())
-
-        @pl.when(place.stage == stage)
-        def _():
-            self.ret_far[rows_of(place.spot), :] = self.ysend[
-                first * LANE_ROWS:(first + 1) * LANE_ROWS, :
-            ]
+
+        def arrive(piece):
+            with jax.named_scope("wait_far"):
+                each(
+                    place.low, place.cell,
+                    lambda step: self.got_far(stage, step, piece).wait_recv(),
+                )
+
+        def leave(piece):
+            each(place.low, place.cell, lambda step: self.back_far(stage, step, piece).start())
+
+            @pl.when(place.inner)
+            def _():
+                self.ret_far[stage, rows_of(place.spot), self.wires(piece)] = self.ysend[
+                    first * LANE_ROWS:(first + 1) * LANE_ROWS, self.wires(piece)
+                ]
+
+        self.serve(first, place.cell, arrive, leave, lambda: None)
 
     def mix(self, meta, ret, wait, store):
         turned = jnp.transpose(meta[...])[:self.tokens, :]
@@ -375,61 +460,75 @@
             return halves(values)
 
         main_mix = [mixing(first, second) for first, second in mains]
-        wait()
-        for part in range(self.parts):
-            low, high = part * self.piece, (part + 1) * self.piece
-            total = jnp.zeros((self.tokens, self.piece), F32)
-            for group, (coarse, fine) in enumerate(main_mix):
-                values = ret[:, group * self.width + low:group * self.width + high]
-                total = total + (mm(coarse, values) + mm(fine, values))
-            coarse, fine = mixing(tails[0] + part, tails[1] + part)
-            values = ret[:, self.base:self.base + self.piece]
-            store(low, high, total + (mm(coarse, values) + mm(fine, values)))
+        tail_mix = [
+            mixing(tails[0] + part, tails[1] + part) for part in range(self.parts)
+        ]
+        for number in range(PIECES):
+            wait(number)
+            at, to = number * self.wire, number * self.step
+            for part in range(self.parts):
+                low, high = part * self.piece, (part + 1) * self.piece
+                coarse, fine = tail_mix[part]
+                values = ret[:, at + self.base:at + self.wire]
+                total = mm(coarse, values) + mm(fine, values)
+                for group, (coarse, fine) in enumerate(main_mix):
+                    start = at + group * self.step
+                    values = ret[:, start + low:start + high]
+                    total = total + (mm(coarse, values) + mm(fine, values))
+                store(number, to + low, to + high, total)
 
     def mix_own(self):
         place = self.place
 
-        def wait():
-            each(1, place.near, lambda distance: self.back_own(distance).wait_recv())
-
-        def store(low, high, value):
+        def wait(piece):
+            with jax.named_scope("wait_back"):
+                each(1, place.near, lambda distance: self.back_here(distance, piece).wait_recv())
+
+        def store(number, low, high, value):
             self.total[:, low:high] = self.total[:, low:high] + value
 
         self.mix(self.meta, self.ret_own, wait, store)
 
     def mix_far(self, stage):
-        @pl.when(self.place.stage == stage)
+        @pl.when(self.place.inner)
         def _():
-            copies = self.back_copies()
-            step = self.width // PIECES
-
-            def wait():
-                self.others(lambda turn: self.returned_far(turn).wait_recv())
-
-            def store(low, high, value):
-                self.far_out[:, low:high] = value.astype(BF16)
-                if high % step == 0:
-                    copies[high // step - 1].start()
-
-            self.mix(self.far_meta, self.ret_far, wait, store)
+            def wait(piece):
+                with jax.named_scope("wait_ret"):
+                    self.others(lambda turn: self.returned_far(stage, turn, piece).wait_recv())
+
+            def store(number, low, high, value):
+                self.far_out[stage, :, low:high] = value.astype(BF16)
+                if high == (number + 1) * self.step:
+                    self.result_to(stage, number).start()
+
+            self.mix(self.far_meta.at[stage], self.ret_far.at[stage], wait, store)
 
     def close(self):
-        step = self.width // PIECES
-        for number, copy in enumerate(self.back_copies()):
-            copy.wait_recv()
-            columns = slice(number * step, (number + 1) * step)
+        place = self.place
+        for piece in range(PIECES):
+            with jax.named_scope("wait_result"):
+                self.result_to(0, piece).wait_recv()
+            columns = self.columns(piece)
             self.out_ref[:, columns] = (
                 self.total[:, columns] + self.far_in[:, columns].astype(F32)
             ).astype(BF16)
-        place = self.place
-        each(1, place.near, lambda distance: self.go_own(distance).wait_send())
-        each(1, place.near, lambda distance: self.back_own(distance).wait_send())
-        self.others(lambda turn: self.go_far(turn).wait_send())
-        for stage in range(place.depth):
-            low = jnp.where(place.stage == stage, 1, 0)
-            each(low, place.cell, lambda step: self.back_far(stage, step).wait_send())
-        for copy in self.block_copies() + self.back_copies():
-            copy.wait_send()
+        self.meta_copy().wait_send()
+        for piece in range(PIECES):
+            self.block_to(0, piece).wait_send()
+            each(1, place.near, lambda distance: self.go_own(distance, piece).wait_send())
+            each(1, place.near, lambda distance: self.back_own(distance, piece).wait_send())
+            for stage in range(place.depth):
+                each(
+                    place.low, place.cell,
+                    lambda step: self.back_far(stage, step, piece).wait_send(),
+                )
+
+        @pl.when(place.inner)
+        def _():
+            for piece in range(PIECES):
+                for stage in range(place.depth):
+                    self.others(lambda turn: self.go_far(stage, turn, piece).wait_send())
+                    self.result_to(stage, piece).wait_send()
 
 
 STATE_ROWS = 8
@@ -553,14 +652,20 @@
             (place_at.half * span + at, tp_at),
         )
 
-    def total_copy():
-        return remote(total_send, total_recv, tot_send, tot_recv, place_at.partner)
+    low_inner = lower_half & place_at.inner
+    first_inner = (place_at.depth - 1) * place_at.side
+
+    def total_copy(stage):
+        return remote(
+            total_send, total_recv, tot_send.at[stage], tot_recv, place_at.beyond(stage)
+        )
 
     def sends_to(distance):
-        return lower_half | (own_at + distance < span)
+        at = lax.rem(own_at + distance, span)
+        return (own_at + distance < span) | (lower_half & (at >= first_inner))
 
     def takes_from(distance):
-        return lower_half | (own_at >= distance)
+        return (own_at >= distance) | low_inner
 
     def u_copies(target, sender):
         place = pl.ds(pl.multiple_of(sender * own_width, own_width), own_width)
@@ -616,6 +721,9 @@
                     absorb(total_ref, total_max, state_recv.at[distance])
             incoming[...] = total_ref[...]
             incoming_max[...] = total_max[...]
+
+        @pl.when(low_inner)
+        def _():
             absorb(total_ref, total_max, state_send)
             for distance in range(span - 1, 0, -1):
                 @pl.when(own_at < distance)
@@ -632,14 +740,15 @@
                 total_send[low_row + key_dim:low_row + message, :] = jnp.where(
                     row == 0, norm, jnp.where(row == 1, total_max[head], 0.0)
                 )
-            total_copy().start()
+            for stage in range(place_at.depth):
+                total_copy(stage).start()
 
     def take_total():
         @pl.when(jnp.logical_not(lower_half))
         def _():
             incoming[...] = jnp.zeros_like(incoming)
             incoming_max[...] = jnp.full_like(incoming_max, -1e30)
-            total_copy().wait_recv()
+            total_copy(0).wait_recv()
             absorb(incoming, incoming_max, total_recv)
             for distance in range(span - 1, 0, -1):
                 @pl.when(own_at >= distance)
@@ -729,9 +838,10 @@
             def _():
                 state_copy(distance, 1).wait_send()
 
-        @pl.when(lower_half)
+        @pl.when(low_inner)
         def _():
-            total_copy().wait_send()
+            for stage in range(place_at.depth):
+                total_copy(stage).wait_send()
 
         for target in range(tp_count):
             @pl.when(tp_at != target)
@@ -770,10 +880,13 @@
     count = ep_count * tp_count
     top_count = routed_expert_index.shape[1]
     capacity = max(2, 3 * tokens * top_count // (2 * count))
-    wire = capacity * width // LANE_ROWS
+    groups = capacity // LANE_ROWS
+    step = width // PIECES
+    wire = PIECES * (groups * step + step * (capacity - groups * LANE_ROWS) // LANE_ROWS)
     side = max(1, tp_count // CORES)
     near = count // 2
     span = ep_count // 2
+    depth = ep_count // side // 2
     rows = near * capacity
     padded = -(-tokens // 128) * 128
     hidden_width = routed_gate_weight.shape[2]
@@ -790,11 +903,13 @@
     block = pltpu.VMEM((tokens, width), BF16)
     meta = pltpu.VMEM((STATE_ROWS, padded), F32)
     half_slots = pltpu.VMEM((near * LANE_ROWS, wire), BF16)
+    far_slots = pltpu.VMEM((depth, near * LANE_ROWS, wire), BF16)
+    far_block = pltpu.VMEM((depth, tokens, width), BF16)
     slots = pltpu.VMEM((2 * near * LANE_ROWS, wire), BF16)
     moe_scratch = (
-        [block, meta, block, meta]
-        + [half_slots, half_slots, slots, slots, half_slots, half_slots]
-        + [block, block]
+        [block, meta, far_block, pltpu.VMEM((depth, STATE_ROWS, padded), F32)]
+        + [half_slots, far_slots, slots, slots, half_slots, far_slots]
+        + [far_block, block]
         + [
             pltpu.VMEM(array.shape[-2:], BF16)
             for array in (
@@ -807,8 +922,10 @@
             pltpu.VMEM((rows, hidden_width), BF16),
             pltpu.VMEM((rows, width), BF16),
             pltpu.VMEM((tokens, width), F32),
-            dma((6,)), dma((count,)), dma((count,)), dma((count,)), dma((count,)),
-            dma((2 * PIECES + 1,)), dma((2 * PIECES + 1,)),
+            dma((6,)), dma((PIECES, near)), dma((PIECES, count)), dma((PIECES, depth * near)),
+            dma((PIECES, count)), dma((PIECES, near)), dma((PIECES, depth * near)),
+            dma((PIECES,)), dma((depth, PIECES)), dma((depth, PIECES)), dma((PIECES,)),
+            dma, dma((depth,)),
         ]
     )
     message = heads * (key_dim + STATE_ROWS)
@@ -827,7 +944,7 @@
         pltpu.VMEM((tp_count, share // BLK, STATE_ROWS, BLK), F32),
         pltpu.VMEM((share, tp_count * heads * value_dim), BF16),
         pltpu.VMEM((tp_count, share // BLK, STATE_ROWS, BLK), F32),
-        dma, dma((span,)), dma((span,)), dma, dma,
+        dma, dma((span,)), dma((span,)), dma((depth,)), dma,
         dma((tp_count,)), dma((tp_count,)), dma((tp_count,)), dma((tp_count,)),
     ]
 
@@ -843,23 +960,28 @@
         experts = Experts(place, capacity, (*moe_in, moe_out, *scratch[:cut]))
         depth = place.depth
         experts.open()
+        early()
+        experts.meet()
         experts.start()
-        early()
         send_states()
         experts.common()
-        experts.relay(0)
+        for piece in range(PIECES):
+            experts.relay(0, piece)
         experts.serve_own()
-        take_states()
         for stage in range(depth):
+            if stage + 1 < depth:
+                experts.relay(stage + 1, 0)
             experts.serve_far(stage)
             if stage + 1 < depth:
-                experts.relay(stage + 1)
+                for piece in range(1, PIECES):
+                    experts.relay(stage + 1, piece)
             if stage == 0:
+                take_states()
                 take_total()
             walk(blocks * stage // depth, blocks * (stage + 1) // depth)
+            experts.mix_far(stage)
             if stage == 0:
                 experts.mix_own()
-            experts.mix_far(stage)
         late()
         experts.close()
         close()

time: 140 us -> 119 us (0.85)
  Pallas kernels: 135 us -> 114 us
    pallas_call x1, Pallas kernels: 135 us -> 114 us  [on_device(): pl.pallas_call(kernel, out_shape=(jax.ShapeDtypeStruct((share, width), BF...]
where the time goes in v2:
time: 119 us
  Pallas kernels  114 us (96%)
  local copies, waits for them, and re-layouts  4.39 us (4%)
    pallas_call x1, Pallas kernels, on_device(): pl.pallas_call(kernel, out_shape=(jax.ShapeDtypeStruct((share, width), BF...  114 us
    unnamed x2, local copies, waits for them, and re-layouts  4.39 us

profile of v2, /device:TPU:0, one launch (start us, length us, event | category | flops | bytes accessed | tf_op | source)
XLA Modules:
  0.0 119.2 jit_solution(3247052170146250378)
XLA Ops:
  0.6 114.1 %both.1 = (bf16[256,2048]{1,0:T(8,128)(2,1)}, bf16[192,2048]{1,0:T(8,128)(2,1)}) custom-call(bf16[1024,128]{1,0:T(8,128)(2,1)} %refs_0_.1, bf16[1024,128]{1,0:T(8,128)(2,1)} %refs_1_.1, bf16[1024,256]{1,0:T(8,128)(2,1)} %refs_2_.1, f32[2,1024]{1,0:T(2,128)} %bitcast.8, f32[2,1024]{1,0:T(2,128)} %bitcast.9, f32[1,2]{1,0:T(1,128)} %bitcast.15, ...), custom_call_target="tpu_custom_call" | custom-call | tf_op jit(solution)/shard_map/both/pallas_call | solution.py:989
  114.8 2.3 %copy.24 = bf16[256,2048]{1,0:T(8,128)(2,1)} copy(bf16[256,2048]{1,0:T(8,128)(2,1)} %get-tuple-element.4) | data formatting | bytes 2097152
  117.1 2.1 %copy.25 = bf16[192,2048]{1,0:T(8,128)(2,1)} copy(bf16[192,2048]{1,0:T(8,128)(2,1)} %get-tuple-element.5) | data formatting | bytes 1572864

commit v3 on v2

--- a/solution.py
+++ b/solution.py
@@ -92,9 +92,9 @@
          su_hbm, sd_hbm, self.out_ref, self.normed, self.meta, self.far_block, self.far_meta,
          self.send_own, self.send_far, self.recv, self.ysend, self.ret_own, self.ret_far,
          self.far_out, self.far_in, self.wg, self.wu, self.wd, self.sg, self.su, self.sd, self.xc,
-         self.hc, self.yc, self.total, load_sem, self.go_send, self.go_recv, self.far_send,
+         self.hc, self.yc, self.gates, self.ups, self.total, self.out, load_sem, self.go_send, self.go_recv, self.far_send,
          self.back_send, self.back_recv, self.far_recv, self.over_send, self.over_recv,
-         self.result_send, self.result_recv, self.meta_send, self.meta_recv) = refs
+         self.result_send, self.result_recv, self.meta_send, self.meta_recv, self.out_sem) = refs
         self.place = place
         self.tokens, self.width = self.x_ref.shape
         self.step = self.width // PIECES
@@ -150,9 +150,6 @@
             jnp.where(hit_second, earlier, 0.0), axis=0, keepdims=True
         )
         self.meta[4:6, :tokens] = self.weight_ref[...]
-        for piece in range(PIECES):
-            self.slots(piece, self.normed, self.meta, self.send_own)
-
     def meet(self):
         place = self.place
         pl.semaphore_wait(
@@ -318,6 +315,7 @@
                 self.block_to(0, piece).start()
 
         for piece in range(PIECES):
+            self.slots(piece, self.normed, self.meta, self.send_own)
             each(1, place.near, lambda distance: self.go_own(distance, piece).start())
         self.recv[0:LANE_ROWS, :] = self.send_own[rows_of(place.spot), :]
 
@@ -356,7 +354,7 @@
         for load in self.loads[3:]:
             load.wait()
 
-    def serve(self, first, sources, arrive, leave, between):
+    def serve(self, first, sources, arrive, leave):
         main_rows, tail_rows = sources * LANE_ROWS, sources * self.tail
         low, piece = first * LANE_ROWS, self.piece
         start = self.groups * main_rows
@@ -380,15 +378,22 @@
                     select(part, False),
                     recv[low:low + main_rows, at + self.base:at + self.wire],
                 ).astype(BF16)
-
-        @pl.loop(0, hc.shape[1] // 256)
-        def _(turn):
-            columns = pl.ds(pl.multiple_of(turn * 256, 256), 256)
-            gate = mm(xc[:rows, :], self.wg[:, columns])
-            up = mm(xc[:rows, :], self.wu[:, columns])
-            hc[:rows, columns] = (gate * jax.nn.sigmoid(gate) * up).astype(BF16)
-
-        between()
+            last = number == PIECES - 1
+
+            @pl.loop(0, hc.shape[1] // 256)
+            def _(turn):
+                columns = pl.ds(pl.multiple_of(turn * 256, 256), 256)
+                gate = mm(xc[:rows, to:to + self.step], self.wg[to:to + self.step, columns])
+                up = mm(xc[:rows, to:to + self.step], self.wu[to:to + self.step, columns])
+                if number:
+                    gate = gate + self.gates[:rows, columns]
+                    up = up + self.ups[:rows, columns]
+                if last:
+                    hc[:rows, columns] = (gate * jax.nn.sigmoid(gate) * up).astype(BF16)
+                else:
+                    self.gates[:rows, columns] = gate
+                    self.ups[:rows, columns] = up
+
         for number in range(PIECES):
             at, to = number * self.wire, number * self.step
 
@@ -418,12 +423,24 @@
                 each(1, place.near, lambda distance: self.go_own(distance, piece).wait_recv())
 
         def leave(piece):
-            each(1, place.near, lambda distance: self.back_own(distance, piece).start())
-            self.ret_own[rows_of(place.spot), self.wires(piece)] = self.ysend[
-                0:LANE_ROWS, self.wires(piece)
-            ]
-
-        self.serve(0, place.near, arrive, leave, self.start_outer)
+            if piece == 0:
+                self.start_outer()
+
+        self.serve(0, place.near, arrive, leave)
+
+    def return_own(self, low, high):
+        for piece in range(PIECES):
+            each(low, high, lambda distance: self.back_own(distance, piece).start())
+
+    def return_plane(self):
+        place = self.place
+        self.return_own(1, place.cell)
+        self.ret_own[rows_of(place.spot), :] = self.ysend[0:LANE_ROWS, :]
+
+    def return_planes(self, chosen):
+        @pl.when(chosen)
+        def _():
+            self.return_own(self.place.cell, self.place.near)
 
     def serve_far(self, stage):
         place = self.place
@@ -445,7 +462,7 @@
                     first * LANE_ROWS:(first + 1) * LANE_ROWS, self.wires(piece)
                 ]
 
-        self.serve(first, place.cell, arrive, leave, lambda: None)
+        self.serve(first, place.cell, arrive, leave)
 
     def mix(self, meta, ret, wait, store):
         turned = jnp.transpose(meta[...])[:self.tokens, :]
@@ -503,15 +520,22 @@
 
             self.mix(self.far_meta.at[stage], self.ret_far.at[stage], wait, store)
 
+    def out_copy(self, piece):
+        columns = self.columns(piece)
+        return pltpu.make_async_copy(
+            self.out.at[:, columns], self.out_ref.at[:, columns], self.out_sem.at[piece]
+        )
+
     def close(self):
         place = self.place
         for piece in range(PIECES):
             with jax.named_scope("wait_result"):
                 self.result_to(0, piece).wait_recv()
             columns = self.columns(piece)
-            self.out_ref[:, columns] = (
+            self.out[:, columns] = (
                 self.total[:, columns] + self.far_in[:, columns].astype(F32)
             ).astype(BF16)
+            self.out_copy(piece).start()
         self.meta_copy().wait_send()
         for piece in range(PIECES):
             self.block_to(0, piece).wait_send()
@@ -530,6 +554,9 @@
                     self.others(lambda turn: self.go_far(stage, turn, piece).wait_send())
                     self.result_to(stage, piece).wait_send()
 
+        for piece in range(PIECES):
+            self.out_copy(piece).wait()
+
 
 STATE_ROWS = 8
 
@@ -551,8 +578,8 @@
 
 
 def mixer_parts(place_at, ep_count, tp_count, refs):
-    (q_ref, k_ref, v_ref, in_ref, forget_ref, bias_ref, extra_ref, gate_ref, gain_ref, wo_hbm,
-     out_ref, wo, locals_ref, state_send, state_recv, total_send, total_recv, total_ref,
+    (q_hbm, k_hbm, v_hbm, in_ref, forget_ref, bias_ref, extra_ref, gate_hbm, gain_ref, wo_hbm,
+     out_hbm, q_ref, k_ref, v_ref, gate_ref, out_ref, in_sem, out_sem, wo, locals_ref, state_send, state_recv, total_send, total_recv, total_ref,
      total_max, incoming, incoming_max, u_ref, squares_ref,
      u_recv, squares_recv, wo_sem, st_send, st_recv, tot_send, tot_recv, us_send, us_recv, sq_send, sq_recv) = refs
     exact = lax.Precision.HIGHEST
@@ -586,6 +613,23 @@
         values = v_ref[at * BLK:(at + 1) * BLK, head * value_dim:(head + 1) * value_dim]
         return jnp.concatenate([values, jnp.ones((BLK, value_dim), BF16)], axis=1)
 
+    inputs = [
+        pltpu.make_async_copy(source, target, in_sem.at[number])
+        for number, (source, target) in enumerate(
+            [(k_hbm, k_ref), (v_hbm, v_ref), (q_hbm, q_ref), (gate_hbm, gate_ref)]
+        )
+    ]
+
+    def fetch():
+        for copy in inputs:
+            copy.start()
+
+    def out_copy(at):
+        rows = slice(at * BLK, (at + 1) * BLK)
+        return pltpu.make_async_copy(
+            out_ref.at[rows, :], out_hbm.at[rows, :], out_sem.at[at]
+        )
+
     found = {}
 
     def grow(state, number):
@@ -604,6 +648,8 @@
 
     def early():
         load.start()
+        for copy in inputs:
+            copy.wait()
         logits = block_rows(forget_ref, lambda value, head: value + bias_ref[:, head:head + 1])
         kept = jnp.minimum(logits, 0.0) - log_one_plus(jnp.exp(-jnp.abs(logits)))
         kept = kept + block_rows(extra_ref)
@@ -796,18 +842,27 @@
                 states[head] = grow(states[head], number)
             squares_ref[at // share_blocks, at % share_blocks] = squares
             if at % share_blocks == share_blocks - 1:
-                target = at // share_blocks
-
-                @pl.when(tp_at != target)
+                @pl.when(jnp.logical_not(place_at.inner))
                 def _():
-                    for copy in u_copies(target, tp_at):
-                        copy.start()
-
-                @pl.when(tp_at == target)
-                def _():
-                    place = pl.ds(pl.multiple_of(tp_at * own_width, own_width), own_width)
-                    u_recv[:, place] = u_ref[target * share:(target + 1) * share, :]
-                    squares_recv[tp_at] = squares_ref[target]
+                    send_share(at // share_blocks)
+
+    def send_share(target):
+        @pl.when(tp_at != target)
+        def _():
+            for copy in u_copies(target, tp_at):
+                copy.start()
+
+        @pl.when(tp_at == target)
+        def _():
+            place = pl.ds(pl.multiple_of(tp_at * own_width, own_width), own_width)
+            u_recv[:, place] = u_ref[target * share:(target + 1) * share, :]
+            squares_recv[tp_at] = squares_ref[target]
+
+    def send_u():
+        @pl.when(place_at.inner)
+        def _():
+            for target in range(tp_count):
+                send_share(target)
 
     def late():
         for sender in range(tp_count):
@@ -831,8 +886,12 @@
                 product = mm(u_recv[at * BLK:(at + 1) * BLK, :], wo[:, place])
                 out_ref[at * BLK:(at + 1) * BLK, place] = (product * inverse).astype(BF16)
 
+            out_copy(at).start()
+
 
     def close():
+        for at in range(share_blocks):
+            out_copy(at).wait()
         for distance in range(1, span):
             @pl.when(sends_to(distance))
             def _():
@@ -849,7 +908,7 @@
                 for copy in u_copies(target, tp_at):
                     copy.wait_send()
 
-    return early, send_states, take_states, take_total, walk, late, close
+    return fetch, early, send_u, send_states, take_states, take_total, walk, late, close
 
 
 def on_device(
@@ -921,15 +980,23 @@
             pltpu.VMEM((rows, width), BF16),
             pltpu.VMEM((rows, hidden_width), BF16),
             pltpu.VMEM((rows, width), BF16),
+            pltpu.VMEM((rows, hidden_width), F32),
+            pltpu.VMEM((rows, hidden_width), F32),
             pltpu.VMEM((tokens, width), F32),
+            block,
             dma((6,)), dma((PIECES, near)), dma((PIECES, count)), dma((PIECES, depth * near)),
             dma((PIECES, count)), dma((PIECES, near)), dma((PIECES, depth * near)),
             dma((PIECES,)), dma((depth, PIECES)), dma((depth, PIECES)), dma((PIECES,)),
-            dma, dma((depth,)),
+            dma, dma((depth,)), dma((PIECES,)),
         ]
     )
     message = heads * (key_dim + STATE_ROWS)
     mixer_scratch = [
+        *[
+            pltpu.VMEM(array.shape, BF16)
+            for array in (queries, head_key_rows, head_value_rows, output_gate_logits)
+        ],
+        pltpu.VMEM((share, width), BF16), dma((4,)), dma((share // BLK,)),
         pltpu.VMEM(mixer_output_weight.shape, BF16),
         pltpu.VMEM((heads * blocks, key_dim, 2 * value_dim), F32),
         pltpu.VMEM((message, value_dim), F32),
@@ -954,20 +1021,22 @@
         scratch = refs[22:]
         cut = len(moe_scratch)
         place = Place(ep_count, tp_count)
-        early, send_states, take_states, take_total, walk, late, close = mixer_parts(
+        fetch, early, send_u, send_states, take_states, take_total, walk, late, close = mixer_parts(
             place, ep_count, tp_count, (*mixer_in, mixer_out, *scratch[cut:])
         )
         experts = Experts(place, capacity, (*moe_in, moe_out, *scratch[:cut]))
         depth = place.depth
+        fetch()
         experts.open()
-        early()
         experts.meet()
         experts.start()
+        early()
         send_states()
         experts.common()
         for piece in range(PIECES):
             experts.relay(0, piece)
         experts.serve_own()
+        experts.return_plane()
         for stage in range(depth):
             if stage + 1 < depth:
                 experts.relay(stage + 1, 0)
@@ -975,13 +1044,16 @@
             if stage + 1 < depth:
                 for piece in range(1, PIECES):
                     experts.relay(stage + 1, piece)
+            else:
+                experts.return_planes(jnp.logical_not(place.inner))
             if stage == 0:
+                experts.return_planes(place.inner)
                 take_states()
                 take_total()
             walk(blocks * stage // depth, blocks * (stage + 1) // depth)
             experts.mix_far(stage)
-            if stage == 0:
-                experts.mix_own()
+        send_u()
+        experts.mix_own()
         late()
         experts.close()
         close()
@@ -992,8 +1064,8 @@
             jax.ShapeDtypeStruct((share, width), BF16),
             jax.ShapeDtypeStruct((tokens, width), BF16),
         ),
-        in_specs=[vmem] * 9 + [hbm] + [vmem] * 4 + [hbm] * 6,
-        out_specs=(vmem, vmem),
+        in_specs=[hbm] * 3 + [vmem] * 4 + [hbm, vmem, hbm] + [vmem] * 4 + [hbm] * 6,
+        out_specs=(hbm, hbm),
         scratch_shapes=moe_scratch + mixer_scratch,
         compiler_params=pltpu.CompilerParams(
             collective_id=0, has_side_effects=True, vmem_limit_bytes=62 * 1024 * 1024

time: 119 us -> 105 us (0.88)
  Pallas kernels: 114 us -> 99.8 us
    pallas_call x1, Pallas kernels: 114 us -> 99.8 us  [on_device(): pl.pallas_call(kernel, out_shape=(jax.ShapeDtypeStruct((share, width), BF...]
where the time goes in v3:
time: 105 us
  Pallas kernels  99.8 us (95%)
  local copies, waits for them, and re-layouts  4.39 us (4%)
    pallas_call x1, Pallas kernels, on_device(): pl.pallas_call(kernel, out_shape=(jax.ShapeDtypeStruct((share, width), BF...  99.8 us
    unnamed x2, local copies, waits for them, and re-layouts  4.39 us

profile of v3, /device:TPU:0, one launch (start us, length us, event | category | flops | bytes accessed | tf_op | source)
XLA Modules:
  0.0 104.8 jit_solution(6751575190827681256)
XLA Ops:
  0.6 99.8 %both.1 = (bf16[256,2048]{1,0:T(8,128)(2,1)}, bf16[192,2048]{1,0:T(8,128)(2,1)}) custom-call(bf16[1024,128]{1,0:T(8,128)(2,1)} %refs_0_.1, bf16[1024,128]{1,0:T(8,128)(2,1)} %refs_1_.1, bf16[1024,256]{1,0:T(8,128)(2,1)} %refs_2_.1, f32[2,1024]{1,0:T(2,128)} %bitcast.8, f32[2,1024]{1,0:T(2,128)} %bitcast.9, f32[1,2]{1,0:T(1,128)} %bitcast.15, ...), custom_call_target="tpu_custom_call" | custom-call | tf_op jit(solution)/shard_map/both/pallas_call | solution.py:1061
  100.4 2.3 %copy.24 = bf16[256,2048]{1,0:T(8,128)(2,1)} copy(bf16[256,2048]{1,0:T(8,128)(2,1)} %get-tuple-element.4) | data formatting | bytes 2097152
  102.7 2.1 %copy.25 = bf16[192,2048]{1,0:T(8,128)(2,1)} copy(bf16[192,2048]{1,0:T(8,128)(2,1)} %get-tuple-element.5) | data formatting | bytes 1572864

commit v4 on v3

--- a/solution.py
+++ b/solution.py
@@ -93,7 +93,7 @@
          self.send_own, self.send_far, self.recv, self.ysend, self.ret_own, self.ret_far,
          self.far_out, self.far_in, self.wg, self.wu, self.wd, self.sg, self.su, self.sd, self.xc,
          self.hc, self.yc, self.gates, self.ups, self.total, self.out, load_sem, self.go_send, self.go_recv, self.far_send,
-         self.back_send, self.back_recv, self.far_recv, self.over_send, self.over_recv,
+         self.far_got, self.far_back, self.back_send, self.back_recv, self.far_recv, self.over_send, self.over_recv,
          self.result_send, self.result_recv, self.meta_send, self.meta_recv, self.out_sem) = refs
         self.place = place
         self.tokens, self.width = self.x_ref.shape
@@ -218,14 +218,14 @@
         columns = self.columns(piece)
         return remote(
             self.normed.at[:, columns], self.far_block.at[stage, :, columns],
-            self.over_send.at[piece], self.over_recv.at[stage, piece], self.place.proxy,
+            self.over_send, self.over_recv.at[stage, piece], self.place.proxy,
         )
 
     def result_to(self, stage, piece):
         columns = self.columns(piece)
         return remote(
             self.far_out.at[stage, :, columns], self.far_in.at[:, columns],
-            self.result_send.at[stage, piece], self.result_recv.at[piece],
+            self.result_send, self.result_recv.at[piece],
             self.place.beyond(stage),
         )
 
@@ -234,7 +234,7 @@
         wires = self.wires(piece)
         return remote(
             self.send_own.at[rows_of(spot), wires], self.recv.at[rows_of(distance), wires],
-            self.go_send.at[piece, distance], self.go_recv.at[piece, distance], device,
+            self.go_send, self.go_recv.at[piece], device,
         )
 
     def back_own(self, distance, piece):
@@ -243,17 +243,11 @@
         return remote(
             self.ysend.at[rows_of(distance), wires],
             self.ret_own.at[rows_of(self.place.spot), wires],
-            self.back_send.at[piece, distance], self.back_recv.at[piece, distance], device,
-        )
-
-    def back_here(self, distance, piece):
-        _, spot = self.place.away(distance, 1)
-        wires = self.wires(piece)
-        return remote(
-            self.ysend.at[rows_of(distance), wires], self.ret_own.at[rows_of(spot), wires],
-            self.back_send.at[piece, distance], self.back_recv.at[piece, distance],
-            self.place.proxy,
-        )
+            self.back_send, self.back_recv.at[piece], device,
+        )
+
+    def all_of(self, source, target, send_sem, recv_sem):
+        return remote(source, target, send_sem, recv_sem, self.place.proxy)
 
     def go_far(self, stage, turn, piece):
         place = self.place
@@ -263,16 +257,7 @@
         wires = self.wires(piece)
         return remote(
             self.send_far.at[stage, rows_of(spot), wires], self.recv.at[rows_of(slot), wires],
-            self.far_send.at[piece, stage * place.near + turn], self.go_recv.at[piece, slot],
-            device,
-        )
-
-    def got_far(self, stage, step, piece):
-        slot = self.place.near + stage * self.place.cell + step
-        wires = self.wires(piece)
-        return remote(
-            self.send_far.at[stage, rows_of(0), wires], self.recv.at[rows_of(slot), wires],
-            self.far_send.at[piece, 0], self.go_recv.at[piece, slot], self.place.proxy,
+            self.far_send, self.far_got.at[stage, piece], device,
         )
 
     def back_far(self, stage, step, piece):
@@ -284,20 +269,7 @@
         return remote(
             self.ysend.at[rows_of(slot), wires],
             self.ret_far.at[stage, rows_of(place.spot), wires],
-            self.back_send.at[piece, slot],
-            self.far_recv.at[piece, stage * place.near + place.level * place.cell + step],
-            device,
-        )
-
-    def returned_far(self, stage, turn, piece):
-        place = self.place
-        level, step = turn // place.cell, lax.rem(turn, place.cell)
-        _, spot = place.at(level, *place.across(step, 1))
-        wires = self.wires(piece)
-        return remote(
-            self.ysend.at[rows_of(0), wires], self.ret_far.at[stage, rows_of(spot), wires],
-            self.back_send.at[piece, 0], self.far_recv.at[piece, stage * place.near + turn],
-            place.proxy,
+            self.far_back, self.far_recv.at[stage, piece], device,
         )
 
     def others(self, work):
@@ -420,7 +392,8 @@
 
         def arrive(piece):
             with jax.named_scope("wait_own"):
-                each(1, place.near, lambda distance: self.go_own(distance, piece).wait_recv())
+                region = self.recv.at[LANE_ROWS:place.near * LANE_ROWS, self.wires(piece)]
+                self.all_of(region, region, self.go_send, self.go_recv.at[piece]).wait_recv()
 
         def leave(piece):
             if piece == 0:
@@ -448,10 +421,14 @@
 
         def arrive(piece):
             with jax.named_scope("wait_far"):
-                each(
-                    place.low, place.cell,
-                    lambda step: self.got_far(stage, step, piece).wait_recv(),
-                )
+                for inner, count in ((True, place.cell - 1), (False, place.cell)):
+                    @pl.when(place.inner == inner)
+                    def _():
+                        end = (first + place.cell) * LANE_ROWS
+                        region = self.recv.at[end - count * LANE_ROWS:end, self.wires(piece)]
+                        self.all_of(
+                            region, region, self.far_send, self.far_got.at[stage, piece]
+                        ).wait_recv()
 
         def leave(piece):
             each(place.low, place.cell, lambda step: self.back_far(stage, step, piece).start())
@@ -499,7 +476,8 @@
 
         def wait(piece):
             with jax.named_scope("wait_back"):
-                each(1, place.near, lambda distance: self.back_here(distance, piece).wait_recv())
+                region = self.ret_own.at[LANE_ROWS:place.near * LANE_ROWS, self.wires(piece)]
+                self.all_of(region, region, self.back_send, self.back_recv.at[piece]).wait_recv()
 
         def store(number, low, high, value):
             self.total[:, low:high] = self.total[:, low:high] + value
@@ -511,7 +489,12 @@
         def _():
             def wait(piece):
                 with jax.named_scope("wait_ret"):
-                    self.others(lambda turn: self.returned_far(stage, turn, piece).wait_recv())
+                    region = self.ret_far.at[
+                        stage, LANE_ROWS:self.place.near * LANE_ROWS, self.wires(piece)
+                    ]
+                    self.all_of(
+                        region, region, self.far_back, self.far_recv.at[stage, piece]
+                    ).wait_recv()
 
             def store(number, low, high, value):
                 self.far_out[stage, :, low:high] = value.astype(BF16)
@@ -536,23 +519,24 @@
                 self.total[:, columns] + self.far_in[:, columns].astype(F32)
             ).astype(BF16)
             self.out_copy(piece).start()
+        def sent(region, sem, other):
+            self.all_of(region, region, sem, other).wait_send()
+
+        others = (place.near - 1) * LANE_ROWS
         self.meta_copy().wait_send()
-        for piece in range(PIECES):
-            self.block_to(0, piece).wait_send()
-            each(1, place.near, lambda distance: self.go_own(distance, piece).wait_send())
-            each(1, place.near, lambda distance: self.back_own(distance, piece).wait_send())
-            for stage in range(place.depth):
-                each(
-                    place.low, place.cell,
-                    lambda step: self.back_far(stage, step, piece).wait_send(),
-                )
+        sent(self.normed, self.over_send, self.over_recv.at[0, 0])
+        sent(self.send_own.at[:others, :], self.go_send, self.go_recv.at[0])
+        sent(self.ysend.at[:others, :], self.back_send, self.back_recv.at[0])
+        for inner, count in ((True, place.cell - 1), (False, place.cell)):
+            @pl.when(place.inner == inner)
+            def _():
+                rows = place.depth * count * LANE_ROWS
+                sent(self.ysend.at[:rows, :], self.far_back, self.far_recv.at[0, 0])
 
         @pl.when(place.inner)
         def _():
-            for piece in range(PIECES):
-                for stage in range(place.depth):
-                    self.others(lambda turn: self.go_far(stage, turn, piece).wait_send())
-                    self.result_to(stage, piece).wait_send()
+            sent(self.send_far.at[:, :others, :], self.far_send, self.far_got.at[0, 0])
+            sent(self.far_out, self.result_send, self.result_recv.at[0])
 
         for piece in range(PIECES):
             self.out_copy(piece).wait()
@@ -718,11 +702,11 @@
         return [
             remote(
                 u_ref.at[target * share:(target + 1) * share, :], u_recv.at[:, place],
-                us_send.at[target], us_recv.at[sender], (ep_at, target),
+                us_send, us_recv, (ep_at, target),
             ),
             remote(
                 squares_ref.at[target], squares_recv.at[sender],
-                sq_send.at[target], sq_recv.at[sender], (ep_at, target),
+                sq_send, sq_recv, (ep_at, target),
             ),
         ]
 
@@ -865,11 +849,11 @@
                 send_share(target)
 
     def late():
-        for sender in range(tp_count):
-            @pl.when(tp_at != sender)
-            def _():
-                for copy in u_copies(0, sender):
-                    copy.wait_recv()
+        others = tp_count - 1
+        region = u_recv.at[:, :others * own_width]
+        remote(region, region, us_send, us_recv, place_at.proxy).wait_recv()
+        region = squares_recv.at[:others]
+        remote(region, region, sq_send, sq_recv, place_at.proxy).wait_recv()
         squares = squares_recv[0]
         for sender in range(1, tp_count):
             squares = squares + squares_recv[sender]
@@ -902,13 +886,51 @@
             for stage in range(place_at.depth):
                 total_copy(stage).wait_send()
 
-        for target in range(tp_count):
-            @pl.when(tp_at != target)
-            def _():
-                for copy in u_copies(target, tp_at):
-                    copy.wait_send()
+        region = u_ref.at[:(tp_count - 1) * share, :]
+        remote(region, region, us_send, us_recv, place_at.proxy).wait_send()
+        region = squares_ref.at[:tp_count - 1]
+        remote(region, region, sq_send, sq_recv, place_at.proxy).wait_send()
 
     return fetch, early, send_u, send_states, take_states, take_total, walk, late, close
+
+
+def settle(results):
+    count = len(results)
+    parts = 4
+
+    def kernel(*refs):
+        sources, targets, held = refs[:count], refs[count:2 * count], refs[2 * count:3 * count]
+        in_sem, out_sem = refs[3 * count:]
+        ins, outs = [], []
+        for number in range(count):
+            rows = held[number].shape[0] // parts
+            for part in range(parts):
+                place, at = slice(part * rows, (part + 1) * rows), number * parts + part
+                here = held[number].at[place, :]
+                ins.append(
+                    pltpu.make_async_copy(sources[number].at[place, :], here, in_sem.at[at])
+                )
+                outs.append(
+                    pltpu.make_async_copy(here, targets[number].at[place, :], out_sem.at[at])
+                )
+        for copy in ins:
+            copy.start()
+        for come, leave in zip(ins, outs):
+            come.wait()
+            leave.start()
+        for copy in outs:
+            copy.wait()
+
+    hbm = pl.BlockSpec(memory_space=pl.ANY)
+    sems = pltpu.SemaphoreType.DMA((count * parts,))
+    return pl.pallas_call(
+        kernel,
+        out_shape=tuple(jax.ShapeDtypeStruct(array.shape, array.dtype) for array in results),
+        in_specs=[hbm] * count,
+        out_specs=(hbm,) * count,
+        scratch_shapes=[pltpu.VMEM(array.shape, array.dtype) for array in results] + [sems, sems],
+        name="settle",
+    )(*results)
 
 
 def on_device(
@@ -984,10 +1006,9 @@
             pltpu.VMEM((rows, hidden_width), F32),
             pltpu.VMEM((tokens, width), F32),
             block,
-            dma((6,)), dma((PIECES, near)), dma((PIECES, count)), dma((PIECES, depth * near)),
-            dma((PIECES, count)), dma((PIECES, near)), dma((PIECES, depth * near)),
-            dma((PIECES,)), dma((depth, PIECES)), dma((depth, PIECES)), dma((PIECES,)),
-            dma, dma((depth,)), dma((PIECES,)),
+            dma((6,)), dma, dma((PIECES,)), dma, dma((depth, PIECES)), dma, dma,
+            dma((PIECES,)), dma((depth, PIECES)), dma, dma((depth, PIECES)), dma,
+            dma((PIECES,)), dma, dma((depth,)), dma((PIECES,)),
         ]
     )
     message = heads * (key_dim + STATE_ROWS)
@@ -1012,7 +1033,7 @@
         pltpu.VMEM((share, tp_count * heads * value_dim), BF16),
         pltpu.VMEM((tp_count, share // BLK, STATE_ROWS, BLK), F32),
         dma, dma((span,)), dma((span,)), dma((depth,)), dma,
-        dma((tp_count,)), dma((tp_count,)), dma((tp_count,)), dma((tp_count,)),
+        dma, dma, dma, dma,
     ]
 
     def kernel(*refs):
@@ -1058,7 +1079,7 @@
         experts.close()
         close()
 
-    return pl.pallas_call(
+    results = pl.pallas_call(
         kernel,
         out_shape=(
             jax.ShapeDtypeStruct((share, width), BF16),
@@ -1079,6 +1100,7 @@
         routed_copy_weight.T, routed_gate_weight, routed_up_weight,
         routed_down_weight, shared_gate_weight, shared_up_weight, shared_down_weight,
     )
+    return settle(results)
 
 
 def solution(mesh):

time: 105 us -> 100 us (0.952)
  local copies, waits for them, and re-layouts: 4.39 us -> 0 us
    unnamed x2 -> x0, local copies, waits for them, and re-layouts: 4.39 us -> none
    pallas_call x1, Pallas kernels: 99.8 us -> 96.8 us  [on_device(): pl.pallas_call(kernel, out_shape=(jax.ShapeDtypeStruct((share, width), BF...]
    pallas_call x0 -> x1, Pallas kernels: none -> 2.3 us  [settle(): pl.pallas_call(kernel, out_shape=tuple((jax.ShapeDtypeStruct(array.shape,...]
where the time goes in v4:
time: 100 us; the launch traced here: 99.9 us
  Pallas kernels  99.1 us (99%)
    pallas_call x1, Pallas kernels, on_device(): pl.pallas_call(kernel, out_shape=(jax.ShapeDtypeStruct((share, width), BF...  96.8 us
    pallas_call x1, Pallas kernels, settle(): pl.pallas_call(kernel, out_shape=tuple((jax.ShapeDtypeStruct(array.shape,...  2.3 us

profile of v4, /device:TPU:0, one launch (start us, length us, event | category | flops | bytes accessed | tf_op | source)
XLA Modules:
  0.0 99.9 jit_solution(9376662217691283108)
XLA Ops:
  0.6 96.8 %both.1 = (bf16[256,2048]{1,0:T(8,128)(2,1)}, bf16[192,2048]{1,0:T(8,128)(2,1)}) custom-call(bf16[1024,128]{1,0:T(8,128)(2,1)} %refs_0_.1, bf16[1024,128]{1,0:T(8,128)(2,1)} %refs_1_.1, bf16[1024,256]{1,0:T(8,128)(2,1)} %refs_2_.1, f32[2,1024]{1,0:T(2,128)} %bitcast.8, f32[2,1024]{1,0:T(2,128)} %bitcast.9, f32[1,2]{1,0:T(1,128)} %bitcast.15, ...), custom_call_target="tpu_custom_call" | custom-call | tf_op jit(solution)/shard_map/both/pallas_call | solution.py:1082
  97.4 2.3 %settle.1 = (bf16[256,2048]{1,0:T(8,128)(2,1)}, bf16[192,2048]{1,0:T(8,128)(2,1)}) custom-call(bf16[256,2048]{1,0:T(8,128)(2,1)} %get-tuple-element.4.refs_0_, bf16[192,2048]{1,0:T(8,128)(2,1)} %get-tuple-element.5.refs_1_), custom_call_target="tpu_custom_call" | custom-call | tf_op jit(solution)/shard_map/settle/pallas_call | solution.py:926

commit v5 on v4

--- a/solution.py
+++ b/solution.py
@@ -13,6 +13,7 @@
 LANE_ROWS = 16
 CORES = 2
 PIECES = 2
+RESULTS = 4
 
 
 def mm(left, right):
@@ -88,14 +89,15 @@
 
 class Experts:
     def __init__(self, place, capacity, refs):
-        (self.x_ref, self.gain_ref, self.idx_ref, self.weight_ref, wg_hbm, wu_hbm, wd_hbm, sg_hbm,
+        (x_hbm, self.gain_ref, self.idx_ref, self.weight_ref, wg_hbm, wu_hbm, wd_hbm, sg_hbm,
          su_hbm, sd_hbm, self.out_ref, self.normed, self.meta, self.far_block, self.far_meta,
          self.send_own, self.send_far, self.recv, self.ysend, self.ret_own, self.ret_far,
          self.far_out, self.far_in, self.wg, self.wu, self.wd, self.sg, self.su, self.sd, self.xc,
-         self.hc, self.yc, self.gates, self.ups, self.total, self.out, load_sem, self.go_send, self.go_recv, self.far_send,
+         self.hc, self.yc, self.gates, self.ups, self.total, self.out, self.mixes, self.x_ref, x_sem, load_sem, self.go_send, self.go_recv, self.far_send,
          self.far_got, self.far_back, self.back_send, self.back_recv, self.far_recv, self.over_send, self.over_recv,
          self.result_send, self.result_recv, self.meta_send, self.meta_recv, self.out_sem) = refs
         self.place = place
+        self.x_load = pltpu.make_async_copy(x_hbm, self.x_ref, x_sem)
         self.tokens, self.width = self.x_ref.shape
         self.step = self.width // PIECES
         self.groups = capacity // LANE_ROWS
@@ -114,8 +116,7 @@
 
     def open(self):
         place, tokens = self.place, self.tokens
-        for load in self.loads:
-            load.start()
+        self.x_load.start()
         barrier = pltpu.get_barrier_semaphore()
 
         def greet(device):
@@ -131,6 +132,9 @@
             for stage in range(1, place.depth):
                 greet(place.beyond(stage))
 
+        for load in self.loads:
+            load.start()
+        self.x_load.wait()
         floats = self.x_ref[...].astype(F32)
         inverse = lax.rsqrt(jnp.mean(floats * floats, axis=1, keepdims=True) + 1e-6)
         self.normed[...] = (floats * inverse * self.gain_ref[...]).astype(BF16)
@@ -221,8 +225,12 @@
             self.over_send, self.over_recv.at[stage, piece], self.place.proxy,
         )
 
+    def result_columns(self, piece):
+        step = self.width // RESULTS
+        return slice(piece * step, (piece + 1) * step)
+
     def result_to(self, stage, piece):
-        columns = self.columns(piece)
+        columns = self.result_columns(piece)
         return remote(
             self.far_out.at[stage, :, columns], self.far_in.at[:, columns],
             self.result_send, self.result_recv.at[piece],
@@ -398,28 +406,29 @@
         def leave(piece):
             if piece == 0:
                 self.start_outer()
+            self.return_own(piece, 1, place.cell)
+            self.ret_own[rows_of(place.spot), self.wires(piece)] = self.ysend[
+                0:LANE_ROWS, self.wires(piece)
+            ]
 
         self.serve(0, place.near, arrive, leave)
 
-    def return_own(self, low, high):
-        for piece in range(PIECES):
-            each(low, high, lambda distance: self.back_own(distance, piece).start())
-
-    def return_plane(self):
-        place = self.place
-        self.return_own(1, place.cell)
-        self.ret_own[rows_of(place.spot), :] = self.ysend[0:LANE_ROWS, :]
+    def return_own(self, piece, low, high):
+        each(low, high, lambda distance: self.back_own(distance, piece).start())
 
     def return_planes(self, chosen):
         @pl.when(chosen)
         def _():
-            self.return_own(self.place.cell, self.place.near)
+            for piece in range(PIECES):
+                self.return_own(piece, self.place.cell, self.place.near)
 
     def serve_far(self, stage):
         place = self.place
         first = place.near + stage * place.cell
 
         def arrive(piece):
+            if piece and stage:
+                self.mix_far(stage - 1, piece)
             with jax.named_scope("wait_far"):
                 for inner, count in ((True, place.cell - 1), (False, place.cell)):
                     @pl.when(place.inner == inner)
@@ -441,80 +450,78 @@
 
         self.serve(first, place.cell, arrive, leave)
 
-    def mix(self, meta, ret, wait, store):
+    def weigh(self, meta):
         turned = jnp.transpose(meta[...])[:self.tokens, :]
         whole = turned.astype(jnp.int32)
         mains, tails = self.keys(*[whole[:, row:row + 1] for row in range(4)])
         slot_lanes = iota((self.tokens, self.place.near * LANE_ROWS), 1)
-
-        def mixing(first, second):
+        spots = mains + [(tails[0] + part, tails[1] + part) for part in range(self.parts)]
+        for number, (first, second) in enumerate(spots):
             values = jnp.where(slot_lanes == first, turned[:, 4:5], 0.0) + jnp.where(
                 slot_lanes == second, turned[:, 5:6], 0.0
             )
-            return halves(values)
-
-        main_mix = [mixing(first, second) for first, second in mains]
-        tail_mix = [
-            mixing(tails[0] + part, tails[1] + part) for part in range(self.parts)
-        ]
-        for number in range(PIECES):
-            wait(number)
-            at, to = number * self.wire, number * self.step
-            for part in range(self.parts):
-                low, high = part * self.piece, (part + 1) * self.piece
-                coarse, fine = tail_mix[part]
-                values = ret[:, at + self.base:at + self.wire]
-                total = mm(coarse, values) + mm(fine, values)
-                for group, (coarse, fine) in enumerate(main_mix):
-                    start = at + group * self.step
-                    values = ret[:, start + low:start + high]
-                    total = total + (mm(coarse, values) + mm(fine, values))
-                store(number, to + low, to + high, total)
+            self.mixes[number, 0], self.mixes[number, 1] = halves(values)
+
+    def mix(self, number, ret, store):
+        at, to = number * self.wire, number * self.step
+
+        def weighted(spot, values):
+            return mm(self.mixes[spot, 0], values) + mm(self.mixes[spot, 1], values)
+
+        for part in range(self.parts):
+            low, high = part * self.piece, (part + 1) * self.piece
+            total = weighted(self.groups + part, ret[:, at + self.base:at + self.wire])
+            for group in range(self.groups):
+                start = at + group * self.step
+                total = total + weighted(group, ret[:, start + low:start + high])
+            store(to + low, to + high, total)
 
     def mix_own(self):
         place = self.place
-
-        def wait(piece):
+        self.weigh(self.meta)
+
+        def store(low, high, value):
+            self.total[:, low:high] = self.total[:, low:high] + value
+
+        for piece in range(PIECES):
             with jax.named_scope("wait_back"):
                 region = self.ret_own.at[LANE_ROWS:place.near * LANE_ROWS, self.wires(piece)]
                 self.all_of(region, region, self.back_send, self.back_recv.at[piece]).wait_recv()
-
-        def store(number, low, high, value):
-            self.total[:, low:high] = self.total[:, low:high] + value
-
-        self.mix(self.meta, self.ret_own, wait, store)
-
-    def mix_far(self, stage):
+            self.mix(piece, self.ret_own, store)
+
+    def mix_far(self, stage, piece):
         @pl.when(self.place.inner)
         def _():
-            def wait(piece):
-                with jax.named_scope("wait_ret"):
-                    region = self.ret_far.at[
-                        stage, LANE_ROWS:self.place.near * LANE_ROWS, self.wires(piece)
-                    ]
-                    self.all_of(
-                        region, region, self.far_back, self.far_recv.at[stage, piece]
-                    ).wait_recv()
-
-            def store(number, low, high, value):
+            if piece == 0:
+                self.weigh(self.far_meta.at[stage])
+
+            def store(low, high, value):
                 self.far_out[stage, :, low:high] = value.astype(BF16)
-                if high == (number + 1) * self.step:
-                    self.result_to(stage, number).start()
-
-            self.mix(self.far_meta.at[stage], self.ret_far.at[stage], wait, store)
+                step = self.width // RESULTS
+                if high % step == 0:
+                    self.result_to(stage, high // step - 1).start()
+
+            with jax.named_scope("wait_ret"):
+                region = self.ret_far.at[
+                    stage, LANE_ROWS:self.place.near * LANE_ROWS, self.wires(piece)
+                ]
+                self.all_of(
+                    region, region, self.far_back, self.far_recv.at[stage, piece]
+                ).wait_recv()
+            self.mix(piece, self.ret_far.at[stage], store)
 
     def out_copy(self, piece):
-        columns = self.columns(piece)
+        columns = self.result_columns(piece)
         return pltpu.make_async_copy(
             self.out.at[:, columns], self.out_ref.at[:, columns], self.out_sem.at[piece]
         )
 
     def close(self):
         place = self.place
-        for piece in range(PIECES):
+        for piece in range(RESULTS):
             with jax.named_scope("wait_result"):
                 self.result_to(0, piece).wait_recv()
-            columns = self.columns(piece)
+            columns = self.result_columns(piece)
             self.out[:, columns] = (
                 self.total[:, columns] + self.far_in[:, columns].astype(F32)
             ).astype(BF16)
@@ -538,7 +545,7 @@
             sent(self.send_far.at[:, :others, :], self.far_send, self.far_got.at[0, 0])
             sent(self.far_out, self.result_send, self.result_recv.at[0])
 
-        for piece in range(PIECES):
+        for piece in range(RESULTS):
             self.out_copy(piece).wait()
 
 
@@ -969,6 +976,7 @@
     span = ep_count // 2
     depth = ep_count // side // 2
     rows = near * capacity
+    spots = groups + LANE_ROWS // (capacity - groups * LANE_ROWS)
     padded = -(-tokens // 128) * 128
     hidden_width = routed_gate_weight.shape[2]
     length = queries.shape[0]
@@ -1006,9 +1014,11 @@
             pltpu.VMEM((rows, hidden_width), F32),
             pltpu.VMEM((tokens, width), F32),
             block,
+            pltpu.VMEM((spots, 2, tokens, near * LANE_ROWS), BF16),
+            block, dma,
             dma((6,)), dma, dma((PIECES,)), dma, dma((depth, PIECES)), dma, dma,
             dma((PIECES,)), dma((depth, PIECES)), dma, dma((depth, PIECES)), dma,
-            dma((PIECES,)), dma, dma((depth,)), dma((PIECES,)),
+            dma((RESULTS,)), dma, dma((depth,)), dma((RESULTS,)),
         ]
     )
     message = heads * (key_dim + STATE_ROWS)
@@ -1047,8 +1057,8 @@
         )
         experts = Experts(place, capacity, (*moe_in, moe_out, *scratch[:cut]))
         depth = place.depth
+        experts.open()
         fetch()
-        experts.open()
         experts.meet()
         experts.start()
         early()
@@ -1057,22 +1067,24 @@
         for piece in range(PIECES):
             experts.relay(0, piece)
         experts.serve_own()
-        experts.return_plane()
         for stage in range(depth):
             if stage + 1 < depth:
                 experts.relay(stage + 1, 0)
+            if stage:
+                experts.mix_far(stage - 1, 0)
             experts.serve_far(stage)
             if stage + 1 < depth:
                 for piece in range(1, PIECES):
                     experts.relay(stage + 1, piece)
-            else:
-                experts.return_planes(jnp.logical_not(place.inner))
             if stage == 0:
                 experts.return_planes(place.inner)
                 take_states()
-                take_total()
-            walk(blocks * stage // depth, blocks * (stage + 1) // depth)
-            experts.mix_far(stage)
+        take_total()
+        for piece in range(PIECES):
+            walk(blocks * piece // PIECES, blocks * (piece + 1) // PIECES)
+            if piece + 1 == PIECES:
+                experts.return_planes(jnp.logical_not(place.inner))
+            experts.mix_far(depth - 1, piece)
         send_u()
         experts.mix_own()
         late()
@@ -1085,7 +1097,7 @@
             jax.ShapeDtypeStruct((share, width), BF16),
             jax.ShapeDtypeStruct((tokens, width), BF16),
         ),
-        in_specs=[hbm] * 3 + [vmem] * 4 + [hbm, vmem, hbm] + [vmem] * 4 + [hbm] * 6,
+        in_specs=[hbm] * 3 + [vmem] * 4 + [hbm, vmem, hbm, hbm] + [vmem] * 3 + [hbm] * 6,
         out_specs=(hbm, hbm),
         scratch_shapes=moe_scratch + mixer_scratch,
         compiler_params=pltpu.CompilerParams(

time: 100 us -> 98.2 us (0.982)
  Pallas kernels: 99.1 us -> 96.9 us
    pallas_call x1, Pallas kernels: 96.8 us -> 94.6 us  [on_device(): pl.pallas_call(kernel, out_shape=(jax.ShapeDtypeStruct((share, width), BF...]
where the time goes in v5:
time: 98.2 us; the launch traced here: 97.7 us
  Pallas kernels  96.9 us (99%)
    pallas_call x1, Pallas kernels, on_device(): pl.pallas_call(kernel, out_shape=(jax.ShapeDtypeStruct((share, width), BF...  94.6 us
    pallas_call x1, Pallas kernels, settle(): pl.pallas_call(kernel, out_shape=tuple((jax.ShapeDtypeStruct(array.shape,...  2.3 us

profile of v5, /device:TPU:0, one launch (start us, length us, event | category | flops | bytes accessed | tf_op | source)
XLA Modules:
  0.0 97.7 jit_solution(3671312378883025048)
XLA Ops:
  0.6 94.6 %both.1 = (bf16[256,2048]{1,0:T(8,128)(2,1)}, bf16[192,2048]{1,0:T(8,128)(2,1)}) custom-call(bf16[1024,128]{1,0:T(8,128)(2,1)} %refs_0_.1, bf16[1024,128]{1,0:T(8,128)(2,1)} %refs_1_.1, bf16[1024,256]{1,0:T(8,128)(2,1)} %refs_2_.1, f32[2,1024]{1,0:T(2,128)} %bitcast.8, f32[2,1024]{1,0:T(2,128)} %bitcast.9, f32[1,2]{1,0:T(1,128)} %bitcast.15, ...), custom_call_target="tpu_custom_call" | custom-call | tf_op jit(solution)/shard_map/both/pallas_call | solution.py:1094
  95.2 2.3 %settle.1 = (bf16[256,2048]{1,0:T(8,128)(2,1)}, bf16[192,2048]{1,0:T(8,128)(2,1)}) custom-call(bf16[256,2048]{1,0:T(8,128)(2,1)} %get-tuple-element.4.refs_0_, bf16[192,2048]{1,0:T(8,128)(2,1)} %get-tuple-element.5.refs_1_), custom_call_target="tpu_custom_call" | custom-call | tf_op jit(solution)/shard_map/settle/pallas_call | solution.py:933
